TPU v7x, 32 devices: a whole 2x2x4 slice. The times are simulated.
32 devices in a mesh: sp: 16 (over z, y, x), tp: 2 (over core).
Axes of the slice: x: 2, y: 2, z: 4, core: 2. Of those that a mesh axis runs over, the one named last changes fastest.
Arguments:
- tokens: bfloat16 [2048, 2048], P('sp'), may hold values from -6 to 6
- input_norm_scale: float32 [2048], replicated, may hold values from 0.1 to 1.9
- input_norm_bias: float32 [2048], replicated, may hold values from -2 to 2
- query_projection: bfloat16 [2048, 1024], P('sp', 'tp'), may hold values from -0.125 to 0.125
- key_projection: bfloat16 [2048, 1024], P('sp', 'tp'), may hold values from -0.125 to 0.125
- value_projection: bfloat16 [2048, 1024], P('sp', 'tp'), may hold values from -0.125 to 0.125
- pooling_input_projection: bfloat16 [2048, 1024], P('sp', 'tp'), may hold values from -0.125 to 0.125
- decay_input_weight: bfloat16 [2048, 128], P('sp'), may hold values from -0.125 to 0.125
- rate_input_weight: bfloat16 [2048, 128], P('sp'), may hold values from -0.125 to 0.125
- gate_input_weight: bfloat16 [2048, 256], P('sp'), may hold values from -0.125 to 0.125
- decay_output_weight: bfloat16 [128, 1024], P(None, 'tp'), may hold values from -0.5 to 0.5
- rate_output_weight: bfloat16 [128, 1024], P(None, 'tp'), may hold values from -0.5 to 0.5
- gate_output_weight: bfloat16 [256, 1024], P(None, 'tp'), may hold values from -0.375 to 0.375
- decay_bias_base: float32 [1024], P('tp'), may hold values from -13 to -2.5
- learning_rate_base: float32 [1024], P('tp'), may hold values from -4 to 4
- key_prenorm_scale: float32 [1024], P('tp'), may hold values from 0.1 to 1.9
- key_learning_scale: float32 [1024], P('tp'), may hold values from 0.1 to 1.9
- self_term_weight: float32 [1024], P('tp'), may hold values from -3 to 3
- head_norm_scale: float32 [1024], P('tp'), may hold values from 0.1 to 1.9
- head_norm_bias: float32 [1024], P('tp'), may hold values from -3 to 3
- rate_extra_log: float32 [2048, 1024], P('sp', 'tp'), may hold values from -0.7 to 0.7
- decay_extra_log: float32 [2048, 1024], P('sp', 'tp'), may hold values from -0.7 to 0
- starting_head_state: float32 [16, 64, 64], P('tp'), may hold values from -12 to 12
- pooling_group_matrix: bfloat16 [8, 128, 128], P('tp'), may hold values from -0.5 to 0.5
- pooling_output_scale: float32 [1024], P('tp'), may hold values from 0.1 to 1.9
- output_attention_rows: bfloat16 [1024, 2048], P('tp', 'sp'), may hold values from -0.125 to 0.125
- output_pooling_rows: bfloat16 [1024, 2048], P('tp', 'sp'), may hold values from -0.125 to 0.125
Outputs:
- mixed: bfloat16 [2048, 2048], P(('sp', 'tp'))
All inputs are finite; a program needn't handle non-finite values.
Results may differ from a plain program's by a relative error of at most 0.019.
Values may be sent and summed in bfloat16 or wider, within the bound.
A program may use at most 128 MiB of HBM per device.

v0:
```python
import math

import jax
import jax.numpy as jnp
from jax import lax
from jax.sharding import PartitionSpec as P

HEAD_CHANNELS = 64
POOL_GROUPS = 8
POOL_GROUP = 128


pool_windows = (2, 4, 8, 16)
pool_reach = 16
span_most = 64
highest = lax.Precision.HIGHEST


def prefix(x, axis, join, neutral):
    place = lax.axis_index(axis)
    gathered = jax.tree.map(
        lambda a, kind: lax.all_gather(a.astype(kind), axis), x, (jnp.bfloat16, jnp.bfloat16)
    )
    state = jax.tree.map(lambda a, e: jnp.zeros_like(a) + jnp.asarray(e, a.dtype), x, neutral)

    def one(hop, state):
        return join(
            state,
            jax.tree.map(
                lambda a, own: lax.dynamic_index_in_dim(a, hop, 0, False).astype(own.dtype),
                gathered,
                x,
            ),
        )

    return lax.fori_loop(0, place, one, state)


def passed_along(value, axis, steps):
    count = lax.axis_size(axis)
    leading, last = (max(0, -steps), min(count, count - steps))
    return lax.ppermute(value, axis, [(source, source + steps) for source in range(leading, last)])


def compose(earlier, later):
    joined_map = jnp.einsum("hij,hjk->hik", earlier[0], later[0], precision=highest)
    joined_state = jnp.einsum("hij,hjk->hik", earlier[1], later[0], precision=highest) + later[1]
    return (joined_map, joined_state)


def block_recurrence(carry, inputs):
    run_local, run_map = carry
    recv, decay_logarithm, key_t, value_t, alpha_t, beta_t = inputs
    span_len = recv.shape[1]
    total = jnp.cumsum(decay_logarithm, axis=1)
    before = total - decay_logarithm
    rows = jnp.arange(span_len, dtype=jnp.int32)[:, None]
    cols = jnp.arange(span_len, dtype=jnp.int32)[None, :]
    strict = (rows > cols)[None, :, :, None]
    upto = (rows >= cols)[None, :, :, None]
    weight_before = jnp.exp(
        jnp.where(strict, before[:, :, None, :] - total[:, None, :, :], -jnp.inf)
    )
    weight_now = jnp.exp(jnp.where(upto, total[:, :, None, :] - total[:, None, :, :], -jnp.inf))
    lower_a = jnp.einsum("htk,hsk,htsk->hts", alpha_t, beta_t, weight_before, precision=highest)
    lower_b = jnp.einsum("htk,hsk,htsk->hts", alpha_t, key_t, weight_before, precision=highest)
    read_b = jnp.einsum("htk,hsk,htsk->hts", recv, beta_t, weight_now, precision=highest)
    read_k = jnp.einsum("htk,hsk,htsk->hts", recv, key_t, weight_now, precision=highest)
    system = jnp.eye(span_len, dtype=jnp.float32)[None] - lower_a
    a_hat = alpha_t * jnp.exp(before)
    r_hat = recv * jnp.exp(total)
    w_part = jax.scipy.linalg.solve_triangular(system, a_hat, lower=True, unit_diagonal=True)
    u_right = jnp.einsum("hts,hsv->htv", lower_b, value_t, precision=highest)
    u_part = jax.scipy.linalg.solve_triangular(system, u_right, lower=True, unit_diagonal=True)
    y_map = r_hat + jnp.einsum("hts,hsk->htk", read_b, w_part, precision=highest)
    y_local = jnp.einsum("hts,hsv->htv", read_b, u_part, precision=highest) + jnp.einsum(
        "hts,hsv->htv", read_k, value_t, precision=highest
    )
    end_decay = jnp.exp(total[:, -1:, :] - total)
    beta_end = beta_t * end_decay
    key_end = key_t * end_decay
    last_decay = jnp.exp(total[:, -1, :])
    map_block = jnp.eye(last_decay.shape[1], dtype=jnp.float32)[None] * last_decay[
        :, None, :
    ] + jnp.einsum("hsi,hsk->hik", w_part, beta_end, precision=highest)
    local_block = jnp.einsum("hsv,hsk->hvk", u_part, beta_end, precision=highest) + jnp.einsum(
        "hsv,hsk->hvk", value_t, key_end, precision=highest
    )
    out_local = y_local + jnp.einsum("hvk,htk->htv", run_local, y_map, precision=highest)
    out_map = jnp.einsum("hjk,htk->htj", run_map, y_map, precision=highest)
    new_local = jnp.einsum("hvj,hjk->hvk", run_local, map_block, precision=highest) + local_block
    new_map = jnp.einsum("hij,hjk->hik", run_map, map_block, precision=highest)
    return ((new_local, new_map), (out_local, out_map))


def window_width(scale_index):
    result = jnp.zeros(scale_index.shape, jnp.float32)
    for level, width in enumerate(pool_windows):
        result = jnp.where(scale_index == level, jnp.float32(width), result)
    return result


def window_sums(extended, scale_index, row_total):
    running = jnp.zeros((row_total, extended.shape[1]), jnp.float32)
    chosen = jnp.zeros((row_total, extended.shape[1]), jnp.float32)
    for offset in range(pool_reach):
        running = running + extended[pool_reach - offset : pool_reach - offset + row_total]
        for level, width in enumerate(pool_windows):
            if offset + 1 == width:
                chosen = jnp.where(scale_index[None, :] == level, running, chosen)
    return chosen


def on_device(
    tokens,
    input_norm_scale,
    input_norm_bias,
    query_projection,
    key_projection,
    value_projection,
    pooling_input_projection,
    decay_input_weight,
    rate_input_weight,
    gate_input_weight,
    decay_output_weight,
    rate_output_weight,
    gate_output_weight,
    decay_bias_base,
    learning_rate_base,
    key_prenorm_scale,
    key_learning_scale,
    self_term_weight,
    head_norm_scale,
    head_norm_bias,
    rate_extra_log,
    decay_extra_log,
    starting_head_state,
    pooling_group_matrix,
    pooling_output_scale,
    output_attention_rows,
    output_pooling_rows,
):
    f32 = jnp.float32
    bf16 = jnp.bfloat16
    row_total = tokens.shape[0]
    wide = tokens.astype(f32)
    center = jnp.mean(wide, axis=-1, keepdims=True)
    spread = jnp.mean(jnp.square(wide - center), axis=-1, keepdims=True)
    normed = (
        (wide - center) * lax.rsqrt(spread + 1e-05) * input_norm_scale + input_norm_bias
    ).astype(bf16)
    pieces = (
        lax.all_gather(query_projection, "sp", axis=0, tiled=True),
        lax.all_gather(key_projection, "sp", axis=0, tiled=True),
        lax.all_gather(value_projection, "sp", axis=0, tiled=True),
        lax.all_gather(pooling_input_projection, "sp", axis=0, tiled=True),
        lax.all_gather(decay_input_weight, "sp", axis=0, tiled=True),
        lax.all_gather(rate_input_weight, "sp", axis=0, tiled=True),
        lax.all_gather(gate_input_weight, "sp", axis=0, tiled=True),
    )
    totals = tuple((jnp.dot(normed, piece, preferred_element_type=f32) for piece in pieces))
    rounded = [total.astype(bf16) for total in totals]
    decay_low, rate_low, gate_low = (rounded[4], rounded[5], rounded[6])
    recept, keys, values, pool_in = (rounded[0], rounded[1], rounded[2], rounded[3])
    decay_tanh = jnp.tanh(decay_low.astype(f32)).astype(bf16)
    gate_sig = jax.nn.sigmoid(gate_low.astype(f32)).astype(bf16)
    rate_logarithm = (
        -jax.nn.softplus(
            -(
                decay_bias_base
                + jnp.dot(decay_tanh, decay_output_weight, preferred_element_type=f32)
            )
        )
        - 0.5
        + rate_extra_log
    )
    decay_logarithm = -jnp.exp(rate_logarithm) + decay_extra_log
    rate = jax.nn.sigmoid(
        learning_rate_base + jnp.dot(rate_low, rate_output_weight, preferred_element_type=f32)
    )
    gate = jnp.dot(gate_sig, gate_output_weight, preferred_element_type=f32)
    mix_width = recept.shape[1]
    heads_dev = mix_width // HEAD_CHANNELS

    def head_number(array):
        return array.astype(f32).reshape(row_total, heads_dev, HEAD_CHANNELS)

    def channel_heads(vector):
        return vector.reshape(heads_dev, HEAD_CHANNELS)

    key_wide = keys.astype(f32)
    unit = head_number(key_wide * key_prenorm_scale)
    unit = unit * lax.rsqrt(jnp.sum(unit * unit, axis=-1, keepdims=True) + 1e-06)
    effective_key = head_number(key_wide * (1.0 + (rate - 1.0) * key_learning_scale))
    query_per_head, value_per_head = (head_number(recept), head_number(values))
    span_len = math.gcd(span_most, row_total)
    block_count = row_total // span_len

    def blocked(array):
        return array.reshape(block_count, span_len, heads_dev, HEAD_CHANNELS).transpose(0, 2, 1, 3)

    def unblocked(array):
        return array.transpose(0, 2, 1, 3).reshape(row_total, heads_dev, HEAD_CHANNELS)

    identity_map = jnp.broadcast_to(
        jnp.eye(HEAD_CHANNELS, dtype=f32), (heads_dev, HEAD_CHANNELS, HEAD_CHANNELS)
    )
    zero_state = jnp.zeros((heads_dev, HEAD_CHANNELS, HEAD_CHANNELS), f32)
    final, outputs = lax.scan(
        block_recurrence,
        (zero_state, identity_map),
        (
            blocked(query_per_head),
            blocked(head_number(decay_logarithm)),
            blocked(effective_key),
            blocked(value_per_head),
            blocked(-unit),
            blocked(unit * head_number(rate)),
        ),
    )
    local_state, block_map = final
    read_local = unblocked(outputs[0])
    read_map = unblocked(outputs[1])
    prior_map, prior_state = prefix(
        (block_map, local_state), "sp", compose, (identity_map, zero_state)
    )
    entry = (
        jnp.einsum("hvj,hjk->hvk", starting_head_state, prior_map, precision=highest) + prior_state
    )
    reading = read_local + jnp.einsum("hvk,thk->thv", entry, read_map, precision=highest)
    center_h = jnp.mean(reading, axis=-1, keepdims=True)
    spread_h = jnp.mean(jnp.square(reading - center_h), axis=-1, keepdims=True)
    split_by_head = (reading - center_h) * lax.rsqrt(
        spread_h + 1e-05 * HEAD_CHANNELS
    ) * channel_heads(head_norm_scale) + channel_heads(head_norm_bias)
    split_by_head = (
        split_by_head
        + jnp.sum(
            query_per_head * effective_key * channel_heads(self_term_weight), axis=-1, keepdims=True
        )
        * value_per_head
    )
    attn_out = (split_by_head.reshape(row_total, mix_width) * gate).astype(bf16)
    pool_width_dev = pool_in.shape[1]
    groups_dev = pool_width_dev // POOL_GROUP
    previous = passed_along(pool_in[row_total - pool_reach :], "sp", 1)
    extended = jnp.concatenate([previous, pool_in], axis=0).astype(f32)
    group_ids = (
        lax.axis_index("tp") * groups_dev
        + jnp.arange(pool_width_dev, dtype=jnp.int32) // POOL_GROUP
    )
    scale_index = group_ids // (POOL_GROUPS // 4)
    chosen = window_sums(extended, scale_index, row_total)
    position = (lax.axis_index("sp") * row_total + jnp.arange(row_total, dtype=jnp.int32)).astype(
        f32
    )
    counted = jnp.minimum(position[:, None] + 1.0, window_width(scale_index)[None, :])
    pooled = (chosen / counted - pool_in.astype(f32)).astype(bf16)
    grouped = jnp.einsum(
        "tgc,gcd->tgd",
        pooled.reshape(row_total, groups_dev, POOL_GROUP),
        pooling_group_matrix,
        preferred_element_type=f32,
    )
    pool_out = (grouped.reshape(row_total, pool_width_dev) * pooling_output_scale).astype(bf16)
    mix_columns, pool_columns = (
        lax.all_gather(output_attention_rows, "sp", axis=1, tiled=True),
        lax.all_gather(output_pooling_rows, "sp", axis=1, tiled=True),
    )
    mixed = lax.psum_scatter(
        (
            jnp.dot(attn_out, mix_columns, preferred_element_type=f32)
            + jnp.dot(pool_out, pool_columns, preferred_element_type=f32)
        ).astype(jnp.bfloat16),
        "tp",
        scatter_dimension=0,
        tiled=True,
    ).astype(jnp.float32)
    return mixed.astype(bf16)


def solution(mesh):
    in_specs = (
        P("sp", None),
        P(),
        P(),
        P("sp", "tp"),
        P("sp", "tp"),
        P("sp", "tp"),
        P("sp", "tp"),
        P("sp", None),
        P("sp", None),
        P("sp", None),
        P(None, "tp"),
        P(None, "tp"),
        P(None, "tp"),
        P("tp"),
        P("tp"),
        P("tp"),
        P("tp"),
        P("tp"),
        P("tp"),
        P("tp"),
        P("sp", "tp"),
        P("sp", "tp"),
        P("tp", None, None),
        P("tp", None, None),
        P("tp"),
        P("tp", "sp"),
        P("tp", "sp"),
    )
    out_specs = P(("sp", "tp"), None)
    return jax.shard_map(
        on_device, mesh=mesh, in_specs=in_specs, out_specs=out_specs, check_vma=False
    )
```

profile of v0, /device:TPU:11, one launch (start us, length us, event | category | flops | bytes accessed | tf_op | source)
XLA Modules:
  0.0 707.0 jit_solution(16670624327214654191)
XLA Ops:
  12.6 29.2 %all_gather.41 = bf16[2048,128]{1,0:T(8,128)(2,1)S(1)} all-gather(bf16[128,128]{1,0:T(8,128)(2,1)} %param.41), channel_id=1, replica_groups=mesh['sp'=16,'tp'=2] {'sp'}, dimensions={0}, use_global_device_ids=true | all-gather | bytes 557056 | tf_op jit(solution)/shard_map/all_gather | solution.py:158
  42.6 37.0 %all_gather.39 = bf16[2048,128]{1,0:T(8,128)(2,1)S(1)} all-gather(bf16[128,128]{1,0:T(8,128)(2,1)S(1)} %copy-done.18), channel_id=1, replica_groups=mesh['sp'=16,'tp'=2] {'sp'}, dimensions={0}, use_global_device_ids=true | all-gather | bytes 557056 | tf_op jit(solution)/shard_map/all_gather | solution.py:157
  81.4 2.1 fusion.62
  83.6 54.0 %all-gather.12.cloned.1.call-done = bf16[2048,512]{1,0:T(8,128)(2,1)} async-done(((bf16[128,512]{1,0:T(8,128)(2,1)}), bf16[2048,512]{1,0:T(8,128)(2,1)}) %all-gather.12.cloned.1.call-update) | async-done | bytes 2097168 | tf_op jit(solution)/shard_map/all_gather | solution.py:154
  137.6 3.0 fusion.112
  143.9 55.8 %all-gather.14.cloned.1.call-done = bf16[2048,512]{1,0:T(8,128)(2,1)} async-done(((bf16[128,512]{1,0:T(8,128)(2,1)}), bf16[2048,512]{1,0:T(8,128)(2,1)}) %all-gather.14.cloned.1.call-update) | async-done | bytes 2097168 | tf_op jit(solution)/shard_map/all_gather | solution.py:155
  199.7 2.1 fusion.63
  204.8 232.8 %while.30 = (s32[]{:T(128)}, f32[8,64,64]{1,2,0:T(8,128)S(1)}, f32[8,64,64]{1,2,0:T(8,128)}, f32[2,8,64,64]{3,2,1,0:T(8,128)}, f32[2,8,64,64]{3,2,1,0:T(8,128)},...) while((s32[]{:T(128)}, f32[8,64,64]{1,2,0:T(8,128)S(1)}, ...), condition=%wide.region_5.7_spmd.clone, body=%wide.region_3.6_spmd.clone.sunk | while | flops 363262016 | bytes 87281032 | solution.py:209
  206.1 2.1 bitcast_multiply_fusion.10
  208.3 12.2 %select_exponential_fusion.3 = (f32[8,64,64,64]{3,2,1,0:T(8,128)}, f32[8,64,64,64]{3,2,1,0:T(8,128)}) fusion(f32[8,64,64]{2,1,0:T(8,128)S(1)} %copy.229, pred[64,64]{1,0:T(8,128)(4,1)S(1)} %get-tuple-element.343, f32[8,64,64]{2,1,0:T(8,128)S(1)} %copy.230, pred[64,64]{1,0:T(8,128)(4,1)S(1)} %get-tuple-element.346), kind=kLoop, calls=%fused_computation.18.clone.1 | loop fusion | flops 8388608 | bytes 17047552 | tf_op jit(solution)/shard_map/while/body/eval_jaxpr/exp | solution.py:64
  220.4 17.0 %copy.231 = f32[8,64,64,64]{1,2,3,0:T(8,128)} copy(f32[8,64,64,64]{3,2,1,0:T(8,128)} %get-tuple-element.347) | data formatting | bytes 16777216 | tf_op jit(solution)/shard_map/while
  237.5 17.1 %copy.235 = f32[8,64,64,64]{1,2,3,0:T(8,128)} copy(f32[8,64,64,64]{3,2,1,0:T(8,128)} %get-tuple-element.350) | data formatting | bytes 16777216 | tf_op jit(solution)/shard_map/while
  258.3 12.6 %fusion.230 = (f32[8,64,64]{1,2,0:T(8,128)}, f32[8,64,64]{1,2,0:T(8,128)S(1)}, f32[8,64,64]{1,2,0:T(8,128)S(1)}, f32[8,64,64]{1,2,0:T(8,128)S(1)}) fusion(f32[8,64,64,64]{1,2,3,0:T(8,128)} %copy.231, f32[8,64,64]{2,1,0:T(8,128)S(1)} %copy.232, f32[8,64,64]{2,1,0:T(8,128)S(1)} %copy.233, f32[8,64,64]{2,1,0:T(8,128)S(1)} %copy.234, ...), kind=kLoop, calls=%fused_computation.15.clone.1 | loop fusion | flops 25034752 | bytes 17825792 | tf_op jit(solution)/shard_map/while/body/eval_jaxpr/htk,hsk,htsk->hts/dot_general | solution.py:66
  271.1 39.3 %custom-call.10 = f32[8,1,64,64]{2,3,1,0:T(8,128)S(1)} custom-call(f32[8,1,64,64]{3,2,1,0:T(8,128)S(1)} %add_bitcast_fusion.2), custom_call_target="InvertDiagBlocksLowerTriangular" | custom-call | tf_op jit(solution)/shard_map/while/body/eval_jaxpr/jit(_solve_triangular)/vmap()/triangular_solve | solution.py:72
  322.5 2.1 bitcast_multiply_fusion.10
  324.7 12.2 %select_exponential_fusion.3 = (f32[8,64,64,64]{3,2,1,0:T(8,128)}, f32[8,64,64,64]{3,2,1,0:T(8,128)}) fusion(f32[8,64,64]{2,1,0:T(8,128)S(1)} %copy.229, pred[64,64]{1,0:T(8,128)(4,1)S(1)} %get-tuple-element.343, f32[8,64,64]{2,1,0:T(8,128)S(1)} %copy.230, pred[64,64]{1,0:T(8,128)(4,1)S(1)} %get-tuple-element.346), kind=kLoop, calls=%fused_computation.18.clone.1 | loop fusion | flops 8388608 | bytes 17047552 | tf_op jit(solution)/shard_map/while/body/eval_jaxpr/exp | solution.py:64
  336.9 17.0 %copy.231 = f32[8,64,64,64]{1,2,3,0:T(8,128)} copy(f32[8,64,64,64]{3,2,1,0:T(8,128)} %get-tuple-element.347) | data formatting | bytes 16777216 | tf_op jit(solution)/shard_map/while
  353.8 17.0 %copy.235 = f32[8,64,64,64]{1,2,3,0:T(8,128)} copy(f32[8,64,64,64]{3,2,1,0:T(8,128)} %get-tuple-element.350) | data formatting | bytes 16777216 | tf_op jit(solution)/shard_map/while
  374.5 12.6 %fusion.230 = (f32[8,64,64]{1,2,0:T(8,128)}, f32[8,64,64]{1,2,0:T(8,128)S(1)}, f32[8,64,64]{1,2,0:T(8,128)S(1)}, f32[8,64,64]{1,2,0:T(8,128)S(1)}) fusion(f32[8,64,64,64]{1,2,3,0:T(8,128)} %copy.231, f32[8,64,64]{2,1,0:T(8,128)S(1)} %copy.232, f32[8,64,64]{2,1,0:T(8,128)S(1)} %copy.233, f32[8,64,64]{2,1,0:T(8,128)S(1)} %copy.234, ...), kind=kLoop, calls=%fused_computation.15.clone.1 | loop fusion | flops 25034752 | bytes 17825792 | tf_op jit(solution)/shard_map/while/body/eval_jaxpr/htk,hsk,htsk->hts/dot_general | solution.py:66
  387.3 39.3 %custom-call.10 = f32[8,1,64,64]{2,3,1,0:T(8,128)S(1)} custom-call(f32[8,1,64,64]{3,2,1,0:T(8,128)S(1)} %add_bitcast_fusion.2), custom_call_target="InvertDiagBlocksLowerTriangular" | custom-call | tf_op jit(solution)/shard_map/while/body/eval_jaxpr/jit(_solve_triangular)/vmap()/triangular_solve | solution.py:72
  437.7 1.7 copy.135
  442.4 2.3 convolution_convert_fusion
  444.7 3.4 collective-permute-start
  448.1 1.6 fusion.71
  452.1 46.7 %all-gather.26.cloned.1.call-done = bf16[128,64,64]{2,1,0:T(8,128)(2,1)} async-done(((bf16[8,64,64]{2,1,0:T(8,128)(2,1)}), bf16[128,64,64]{2,1,0:T(8,128)(2,1)}) %all-gather.26.cloned.1.call-update) | async-done | bytes 1048592 | tf_op jit(solution)/shard_map/all_gather | solution.py:22
  498.8 62.0 %all-gather.28.cloned.1.call-done = bf16[128,64,64]{2,1,0:T(8,128)(2,1)} async-done(((bf16[8,64,64]{2,1,0:T(8,128)(2,1)}), bf16[128,64,64]{2,1,0:T(8,128)(2,1)}) %all-gather.28.cloned.1.call-update) | async-done | bytes 1048592 | tf_op jit(solution)/shard_map/all_gather | solution.py:22
  560.8 18.0 %while.29 = (s32[]{:T(128)}, f32[8,64,64]{1,2,0:T(8,128)S(1)}, f32[8,64,64]{1,2,0:T(8,128)S(1)}, s32[]{:T(128)}, bf16[16,8,64,64]{3,2,1,0:T(8,128)(2,1)}, /*inde...) while((s32[]{:T(128)}, f32[8,64,64]{1,2,0:T(8,128)S(1)}, f32[8,64,64]{1,2,0:T(8,128)S(1)}, ...), condition=%wide.region_7.9_spmd, body=%wide.region_6.8_spmd.sunk | while | flops 50397188 | bytes 1638539 | solution.py:36
  581.0 42.2 %all-gather.20.cloned.1.call-done = bf16[512,2048]{1,0:T(8,128)(2,1)} async-done(((bf16[512,128]{1,0:T(8,128)(2,1)}), bf16[512,2048]{1,0:T(8,128)(2,1)}) %all-gather.20.cloned.1.call-update) | async-done | bytes 2097168 | tf_op jit(solution)/shard_map/all_gather | solution.py:267
  623.2 2.2 fusion.65
  625.4 61.7 %all-gather.24.cloned.1.call-done = bf16[512,2048]{1,0:T(8,128)(2,1)} async-done(((bf16[512,128]{1,0:T(8,128)(2,1)}), bf16[512,2048]{1,0:T(8,128)(2,1)}) %all-gather.24.cloned.1.call-update) | async-done | bytes 2097168 | tf_op jit(solution)/shard_map/all_gather | solution.py:268
  687.0 2.9 fusion.49
  689.9 10.2 %reduce-scatter.2.cloned.1.call-done = bf16[64,2048]{1,0:T(8,128)(2,1)} async-done(((bf16[128,2048]{1,0:T(8,128)(2,1)}), bf16[64,2048]{1,0:T(8,128)(2,1)}) %reduce-scatter.2.cloned.1.call-update) | async-done | bytes 262160 | tf_op jit(solution)/shard_map/reduce_scatter | solution.py:270
  (260 shorter events, 71.3 us)
Async XLA Ops:
  6.5 616.6 %copy-start = (bf16[256,512]{1,0:T(8,128)(2,1)S(1)}, bf16[256,512]{1,0:T(8,128)(2,1)}, u32[]{:S(2)}) copy-start(bf16[256,512]{1,0:T(8,128)(2,1)} %param.45) | copy-start | bytes 786436
  6.5 35.3 %copy-start.38 = (f32[512]{0:T(512)S(1)}, f32[512]{0:T(512)}, u32[]{:S(2)}) copy-start(f32[512]{0:T(512)} %param.47) | copy-start | bytes 6148
  6.6 74.8 %all-gather.16.cloned.1.call-start = ((), (), s32[]{:S(2)}) async-start(), calls=%async_computation.3 | async-start | bytes 2228224 | tf_op jit(solution)/shard_map/all_gather | solution.py:153
  7.3 130.3 %all-gather.12.cloned.1.call-start = ((), (), s32[]{:S(2)}) async-start(), calls=%async_computation.1 | async-start | bytes 2228224 | tf_op jit(solution)/shard_map/all_gather | solution.py:154
  8.0 191.6 %all-gather.14.cloned.1.call-start = ((), (), s32[]{:S(2)}) async-start(), calls=%async_computation.2 | async-start | bytes 2228224 | tf_op jit(solution)/shard_map/all_gather | solution.py:155
  8.8 433.5 %all-gather.22.cloned.1.call-start = ((), (), s32[]{:S(2)}) async-start(), calls=%async_computation.6 | async-start | bytes 2228224 | tf_op jit(solution)/shard_map/all_gather | solution.py:156
  9.4 438.8 %all-gather.18.cloned.1.call-start = ((), (), s32[]{:S(2)}) async-start(), calls=%async_computation.4 | async-start | bytes 1114112 | tf_op jit(solution)/shard_map/all_gather | solution.py:159
  9.9 488.8 %all-gather.26.cloned.1.call-start = ((), (), s32[]{:S(2)}) async-start(), calls=%async_computation.9 | async-start | bytes 2228224 | tf_op jit(solution)/shard_map/all_gather | solution.py:22
  10.0 194.1 %copy-start.15 = (f32[64,64]{0,1:T(8,128)}, f32[64,64]{0,1:T(8,128)S(1)}, u32[]{:S(2)}) copy-start(f32[64,64]{0,1:T(8,128)S(1)} %fusion.96) | copy-start | bytes 49156
  11.2 188.4 %copy-start.29 = (f32[128]{0:T(128)}, f32[128]{0:T(128)S(1)}, u32[]{:S(2)}) copy-start(f32[128]{0:T(128)S(1)} %broadcast_multiply_fusion.2) | copy-start | bytes 1540
  12.6 187.1 %copy-start.31 = (f32[128]{0:T(128)}, f32[128]{0:T(128)S(1)}, u32[]{:S(2)}) copy-start(f32[128]{0:T(128)S(1)} %add_rsqrt_fusion.2) | copy-start | bytes 1540
  41.9 37.8 %copy-start.33 = (f32[128,512]{1,0:T(8,128)S(1)}, f32[128,512]{1,0:T(8,128)}, u32[]{:S(2)}) copy-start(f32[128,512]{1,0:T(8,128)} %param.54) | copy-start | bytes 786436
  41.9 37.8 %copy-start.34 = (f32[128,512]{1,0:T(8,128)S(1)}, f32[128,512]{1,0:T(8,128)}, u32[]{:S(2)}) copy-start(f32[128,512]{1,0:T(8,128)} %param.53) | copy-start | bytes 786436
  41.9 37.8 %copy-start.36 = (bf16[128,512]{1,0:T(8,128)(2,1)S(1)}, bf16[128,512]{1,0:T(8,128)(2,1)}, u32[]{:S(2)}) copy-start(bf16[128,512]{1,0:T(8,128)(2,1)} %param.43) | copy-start | bytes 393220
  41.9 37.8 %copy-start.39 = (f32[512]{0:T(512)S(1)}, f32[512]{0:T(512)}, u32[]{:S(2)}) copy-start(f32[512]{0:T(512)} %param.46) | copy-start | bytes 6148
  81.4 56.3 %copy-start.23 = (f32[512]{0:T(512)S(1)}, f32[512]{0:T(512)}, u32[]{:S(2)}) copy-start(f32[512]{0:T(512)} %param.48) | copy-start | bytes 6148
  81.4 56.3 %copy-start.24 = (f32[512]{0:T(512)S(1)}, f32[512]{0:T(512)}, u32[]{:S(2)}) copy-start(f32[512]{0:T(512)} %param.49) | copy-start | bytes 6148
  204.8 237.3 %copy-start.26 = (f32[512]{0:T(512)S(1)}, f32[512]{0:T(512)}, u32[]{:S(2)}) copy-start(f32[512]{0:T(512)} %param.52) | copy-start | bytes 6148
  204.8 237.4 %copy-start.27 = (f32[512]{0:T(512)S(1)}, f32[512]{0:T(512)}, u32[]{:S(2)}) copy-start(f32[512]{0:T(512)} %param.51) | copy-start | bytes 6148
  204.8 237.4 %copy-start.28 = (f32[512]{0:T(512)S(1)}, f32[512]{0:T(512)}, u32[]{:S(2)}) copy-start(f32[512]{0:T(512)} %param.50) | copy-start | bytes 6148
  204.8 237.5 %copy-start.20 = (f32[2048]{0:T(1024)S(1)}, f32[2048]{0:T(1024)}, u32[]{:S(2)}) copy-start(f32[2048]{0:T(1024)} %param.35) | copy-start | bytes 24580
  204.8 237.5 %copy-start.22 = (f32[2048]{0:T(1024)S(1)}, f32[2048]{0:T(1024)}, u32[]{:S(2)}) copy-start(f32[2048]{0:T(1024)} %param.34) | copy-start | bytes 24580
  204.8 237.5 %copy-start.30 = (f32[128]{0:T(128)S(1)}, f32[128]{0:T(128)}, u32[]{:S(2)}) copy-start(f32[128]{0:T(128)} %copy-done.29) | copy-start | bytes 1540
  204.8 237.5 %copy-start.32 = (f32[128]{0:T(128)S(1)}, f32[128]{0:T(128)}, u32[]{:S(2)}) copy-start(f32[128]{0:T(128)} %copy-done.31) | copy-start | bytes 1540
  270.8 42.4 %copy-start.1 = (f32[8,64,64]{1,2,0:T(8,128)S(1)}, f32[8,64,64]{1,2,0:T(8,128)}, u32[]{:S(2)}) copy-start(f32[8,64,64]{1,2,0:T(8,128)} %get-tuple-element.357) | copy-start | bytes 393220 | tf_op jit(solution)/shard_map/while
  387.0 42.4 %copy-start.1 = (f32[8,64,64]{1,2,0:T(8,128)S(1)}, f32[8,64,64]{1,2,0:T(8,128)}, u32[]{:S(2)}) copy-start(f32[8,64,64]{1,2,0:T(8,128)} %get-tuple-element.357) | copy-start | bytes 393220 | tf_op jit(solution)/shard_map/while
  439.4 121.4 %all-gather.28.cloned.1.call-start = ((), (), s32[]{:S(2)}) async-start(), calls=%async_computation.10 | async-start | bytes 2228224 | tf_op jit(solution)/shard_map/all_gather | solution.py:22
  440.5 182.7 %all-gather.20.cloned.1.call-start = ((), (), s32[]{:S(2)}) async-start(), calls=%async_computation.5 | async-start | bytes 2228224 | tf_op jit(solution)/shard_map/all_gather | solution.py:267
  441.2 245.8 %all-gather.24.cloned.1.call-start = ((), (), s32[]{:S(2)}) async-start(), calls=%async_computation.7 | async-start | bytes 2228224 | tf_op jit(solution)/shard_map/all_gather | solution.py:268
  442.0 258.2 %reduce-scatter.2.cloned.1.call-start = ((), (), s32[]{:S(2)}) async-start(), calls=%async_computation.8 | async-start | bytes 786432 | tf_op jit(solution)/shard_map/reduce_scatter | solution.py:270
  444.7 6.6 collective-permute-start
  451.3 109.5 %copy-start.16 = (f32[64,64]{0,1:T(8,128)S(1)}, f32[64,64]{0,1:T(8,128)}, u32[]{:S(2)}) copy-start(f32[64,64]{0,1:T(8,128)} %copy-done.15) | copy-start | bytes 49156
  (26 other events, 244.7 us)
Sparse Core Ops, SparseCore 0:
  10.1 62.8 all-gather.15
  75.8 61.7 all-gather.11
  140.4 59.2 all-gather.13
  202.3 59.1 all-gather.21
  264.1 53.8 all-gather.17
  439.5 59.2 all-gather.25
  501.6 59.1 all-gather.27
  563.5 59.6 all-gather.19
  625.9 61.1 all-gather.23
  690.1 10.0 reduce-scatter.1
where the time goes:
time: 711 us; the launch traced here: 707 us
  waiting for transfers between devices  337 us (47%)
  other arithmetic  139 us (20%)
  local copies, waits for them, and re-layouts  93.6 us (13%)
  blocking collectives  66.3 us (9%)
  matrix products  51.3 us (7%)
  between operations  14.1 us (2%)
    all_gather x2, waiting for transfers between devices, prefix(): lax.all_gather(a.astype(kind), axis)  109 us
    another operation x10, other arithmetic, block_recurrence(): jax.scipy.linalg.solve_triangular(system, a_hat, lower=True, unit_diagona...  78.9 us
    while x44, local copies, waits for them, and re-layouts  70 us
    all_gather x1, waiting for transfers between devices, on_device(): lax.all_gather(output_pooling_rows, 'sp', axis=1, tiled=True)  61.7 us
    all_gather x1, waiting for transfers between devices, on_device(): lax.all_gather(value_projection, 'sp', axis=0, tiled=True)  55.8 us
    all_gather x1, waiting for transfers between devices, on_device(): lax.all_gather(key_projection, 'sp', axis=0, tiled=True)  54 us
    all_gather x1, waiting for transfers between devices, on_device(): lax.all_gather(output_attention_rows, 'sp', axis=1, tiled=True)  42.2 us
    all_gather x1, blocking collectives, on_device(): lax.all_gather(decay_input_weight, 'sp', axis=0, tiled=True)  37 us
  transfers between devices with their start and end apart: 11, of which 7 were waited for; matrix products, arithmetic and copies ran while one was open for 40% of the time, Pallas kernels for 0%

commit v1 on v0

v1 whole, which is shorter than its diff:
```python
import functools
import math

import jax
import jax.numpy as jnp
from jax import lax
from jax.experimental import pallas as pl
from jax.experimental.pallas import tpu as pltpu
from jax.sharding import PartitionSpec as P

HEAD_CHANNELS = 64
POOL_GROUPS = 8
POOL_GROUP = 128

pool_windows = (2, 4, 8, 16)
pool_reach = 16
span_most = 64
highest = lax.Precision.HIGHEST
f32 = jnp.float32
bf16 = jnp.bfloat16
MESH = pl.DeviceIdType.MESH
VMEM_LIMIT = 56 * 1024 * 1024

MM = (((1,), (0,)), ((), ()))
MT = (((1,), (1,)), ((), ()))
TM = (((0,), (0,)), ((), ()))


def split(a):
    high = a.astype(bf16)
    return high, (a - high.astype(f32)).astype(bf16)


def dot1(a, b, dims):
    return lax.dot_general(a, b, dims, preferred_element_type=f32)


def mm3(a, b, dims=MM):
    ah, al = split(a)
    bh, bl = split(b)
    return dot1(ah, bh, dims) + (dot1(ah, bl, dims) + dot1(al, bh, dims))


def mm2(a, b, dims=MM):
    ah, al = split(a)
    return dot1(ah, b, dims) + dot1(al, b, dims)


def passed_along(value, axis, steps):
    count = lax.axis_size(axis)
    leading, last = (max(0, -steps), min(count, count - steps))
    return lax.ppermute(value, axis, [(source, source + steps) for source in range(leading, last)])


def remote(src, dst, send, recv, peer):
    return pltpu.make_async_remote_copy(
        src_ref=src, dst_ref=dst, send_sem=send, recv_sem=recv,
        device_id={"sp": peer}, device_id_type=MESH,
    )


def project_kernel(n, group, normed_ref, w_ref, out_ref, nall, wall, res, got,
                   own_sem, ns, nr, ws, wr, rs, rr):
    me = lax.axis_index("sp")
    lo = lax.rem(me, group)
    base = me - lo
    rows = normed_ref.shape[0]
    deep = w_ref.shape[1]
    wide = w_ref.shape[2]
    barrier = pltpu.get_barrier_semaphore()
    for j in range(1, n):
        pl.semaphore_signal(barrier, inc=1, device_id={"sp": lax.rem(me + j, n)}, device_id_type=MESH)
    pl.semaphore_wait(barrier, n - 1)

    def row_slot(index, size):
        return pl.ds(pl.multiple_of(index * size, size), size)

    def w_copy(j):
        peer = lax.rem(me + j, n)
        return remote(w_ref.at[lax.rem(peer, group)], wall.at[row_slot(me, deep)],
                      ws.at[j], wr.at[j], peer)

    def w_land(j):
        source = lax.rem(me + n - j, n)
        return remote(w_ref.at[0], wall.at[row_slot(source, deep)], ws.at[j], wr.at[j], source)

    def n_copy(j):
        return remote(normed_ref, nall.at[row_slot(lo, rows)], ns.at[j], nr.at[j],
                      base + lax.rem(lo + j, group))

    def n_land(j):
        at = lax.rem(lo + group - j, group)
        return remote(normed_ref, nall.at[row_slot(at, rows)], ns.at[j], nr.at[j], base + at)

    for j in range(1, group):
        n_copy(j).start()
    for j in range(1, n):
        w_copy(j).start()
    own = (
        pltpu.make_async_copy(normed_ref, nall.at[row_slot(lo, rows)], own_sem.at[0]),
        pltpu.make_async_copy(w_ref.at[lo], wall.at[row_slot(me, deep)], own_sem.at[1]),
    )
    for c in own:
        c.start()
    for c in own:
        c.wait()
    for j in range(1, group):
        n_land(j).wait_recv()
    for j in range(1, n):
        w_land(j).wait_recv()
    weights = wall[...]
    for j in range(1, group):
        at = lax.rem(lo + j, group)
        part = jnp.dot(nall[row_slot(at, rows), :], weights, preferred_element_type=f32)
        res[j] = part.astype(bf16)
        remote(res.at[j], got.at[j], rs.at[j], rr.at[j], base + at).start()
    got[0] = jnp.dot(normed_ref[...], weights, preferred_element_type=f32).astype(bf16)
    for j in range(1, group):
        n_copy(j).wait_send()
    for j in range(1, n):
        w_copy(j).wait_send()
    for j in range(1, group):
        c = remote(res.at[j], got.at[j], rs.at[j], rr.at[j], base + lax.rem(lo + j, group))
        c.wait_send()
        c.wait_recv()
    for col in range(group):
        out_ref[:, col * wide:(col + 1) * wide] = got[lax.rem(lo + group - col, group)]


def project(normed, weights, n, group):
    rows, width = normed.shape
    _, deep, wide = weights.shape
    dma = pltpu.SemaphoreType.DMA
    return pl.pallas_call(
        functools.partial(project_kernel, n, group),
        out_shape=jax.ShapeDtypeStruct((rows, group * wide), bf16),
        in_specs=[pl.BlockSpec(memory_space=pltpu.VMEM)] * 2,
        out_specs=pl.BlockSpec(memory_space=pltpu.VMEM),
        scratch_shapes=[
            pltpu.VMEM((group * rows, width), bf16),
            pltpu.VMEM((n * deep, wide), bf16),
            pltpu.VMEM((group, rows, wide), bf16),
            pltpu.VMEM((group, rows, wide), bf16),
            dma((2,)),
            dma((group,)), dma((group,)), dma((n,)), dma((n,)), dma((group,)), dma((group,)),
        ],
        compiler_params=pltpu.CompilerParams(
            collective_id=0, has_side_effects=True, vmem_limit_bytes=VMEM_LIMIT
        ),
        cost_estimate=pl.CostEstimate(flops=10**11, bytes_accessed=10**7, transcendentals=0),
        name="project",
    )(normed, weights)


def halves(parts):
    return parts[0] if len(parts) == 1 else jnp.concatenate(parts, axis=1)


def recur_kernel(span, q_ref, k_ref, v_ref, gl_ref, dl_ref, rl_ref, gw_ref, dw_ref, rw_ref,
                 vec_ref, re_ref, de_ref, yl_ref, ym_ref, bonus_ref, gate_ref, ms_ref):
    hc = HEAD_CHANNELS
    T = q_ref.shape[0]
    heads = q_ref.shape[1] // hc
    vec = vec_ref[...]
    dbase, lbase, kscale, klearn, selfw = (vec[i:i + 1] for i in range(5))
    tanh_low = jnp.tanh(dl_ref[...].astype(f32)).astype(bf16)
    z = dbase + jnp.dot(tanh_low, dw_ref[...], preferred_element_type=f32)
    logw = de_ref[...] - jax.nn.sigmoid(z) * jnp.exp(re_ref[...] - 0.5)
    rate = jax.nn.sigmoid(lbase + jnp.dot(rl_ref[...], rw_ref[...], preferred_element_type=f32))
    sig_low = jax.nn.sigmoid(gl_ref[...].astype(f32)).astype(bf16)
    gate_ref[...] = jnp.dot(sig_low, gw_ref[...], preferred_element_type=f32)
    q = q_ref[...].astype(f32)
    k = k_ref[...].astype(f32)
    v = v_ref[...].astype(f32)
    unit = k * kscale
    keff = k * (1.0 + (rate - 1.0) * klearn)
    qkw = q * keff * selfw

    rows = lax.broadcasted_iota(jnp.int32, (T, T), 0)
    cols = lax.broadcasted_iota(jnp.int32, (T, T), 1)
    strict = rows > cols
    upto = rows >= cols
    total = jnp.dot(upto.astype(f32), logw, precision=highest, preferred_element_type=f32)
    before = total - logw
    ending = total[T - 1:T]

    def per(array):
        return [array[:, h * hc:(h + 1) * hc] for h in range(heads)]

    norms = [u * lax.rsqrt(jnp.sum(u * u, axis=1, keepdims=True) + 1e-6) for u in per(unit)]
    unit = halves(norms)
    bonus_ref[...] = halves(
        [jnp.sum(a, axis=1, keepdims=True) * b for a, b in zip(per(qkw), per(v))]
    )
    alpha = -unit
    beta = unit * rate
    center = jnp.concatenate(
        [
            jnp.broadcast_to(total[c + span // 2:c + span // 2 + 1], (span, total.shape[1]))
            for c in range(0, T, span)
        ],
        axis=0,
    )
    down = jnp.exp(center - total)
    fa = jnp.concatenate([alpha * jnp.exp(before - center), q * jnp.exp(total - center)], axis=0)
    fb = jnp.concatenate([beta * down, keff * down], axis=0)
    pair = [mm3(a, b, MT) for a, b in zip(per(fa), per(fb))]
    same = (rows // span) == (cols // span)
    lower = jnp.concatenate(
        [
            jnp.concatenate([same & strict] * 2, axis=1),
            jnp.concatenate([same & upto] * 2, axis=1),
        ],
        axis=0,
    )
    pair = [jnp.where(lower, p, 0.0) for p in pair]
    for edge in range(span, T, span):
        at = total[edge - 1:edge]
        past = jnp.exp(jnp.minimum(at - total, 0.0))
        ga = jnp.concatenate(
            [alpha * jnp.exp(jnp.minimum(before - at, 0.0)), q * jnp.exp(jnp.minimum(total - at, 0.0))],
            axis=0,
        )
        gb = jnp.concatenate([beta * past, keff * past], axis=0)
        cross = ((rows // span) == (edge // span)) & (cols < edge)
        cross = jnp.concatenate([jnp.concatenate([cross] * 2, axis=1)] * 2, axis=0)
        pair = [
            jnp.where(cross, mm3(a, b, MT), p) for a, b, p in zip(per(ga), per(gb), pair)
        ]
    la = [p[:T, :T] for p in pair]
    lb = [p[:T, T:] for p in pair]
    rb = [p[T:, :T] for p in pair]
    rk = [p[T:, T:] for p in pair]

    def joins(size):
        return ((rows // (2 * size)) == (cols // (2 * size))) & ((rows // size) != (cols // size))

    eye = (rows == cols).astype(f32)
    inverse = [eye + jnp.where(joins(1), a, 0.0) for a in la]
    size = 2
    while size < T:
        m = joins(size)
        mid = [mm3(jnp.where(m, a, 0.0), x) for a, x in zip(la, inverse)]
        inverse = [x + mm3(x, y) for x, y in zip(inverse, mid)]
        size *= 2
    ahat = per(alpha * jnp.exp(before))
    rhat = per(q * jnp.exp(total))
    values = [a.astype(bf16) for a in per(v)]
    right = [jnp.concatenate([a, mm2(b, w)], axis=1) for a, b, w in zip(ahat, lb, values)]
    wu = [mm3(x, r) for x, r in zip(inverse, right)]
    y = [mm3(b, r) for b, r in zip(rb, wu)]
    own = [mm2(b, w) for b, w in zip(rk, values)]
    ym_ref[...] = halves([r + a[:, :hc] for r, a in zip(rhat, y)])
    yl_ref[...] = halves([o + a[:, hc:] for o, a in zip(own, y)])
    tail = jnp.exp(ending - total)
    bend = per(beta * tail)
    kend = per(keff * tail)
    ie = lax.broadcasted_iota(jnp.int32, (hc, hc), 0)
    je = lax.broadcasted_iota(jnp.int32, (hc, hc), 1)
    last = per(jnp.exp(ending))
    for h in range(heads):
        both = mm3(wu[h], bend[h], TM)
        kh, kl = split(kend[h])
        added = dot1(values[h], kh, TM) + dot1(values[h], kl, TM)
        grown = jnp.where(ie == je, jnp.broadcast_to(last[h], (hc, hc)), 0.0)
        ms_ref[h] = jnp.concatenate([both[:hc] + grown, both[hc:] + added], axis=0).astype(bf16)


def recur(proj, mix, lows, gw, dw, rw, vec, re, de):
    T = proj.shape[0]
    hc = HEAD_CHANNELS
    block = math.gcd(mix, 256)
    per = block // hc
    grank, drank, rrank = lows
    heads = mix // hc
    at = 4 * mix

    def col(offset, width):
        return pl.BlockSpec((T, width), lambda i: (0, offset // width + i))

    def fixed(offset, width):
        return pl.BlockSpec((T, width), lambda i: (0, offset // width))

    def weight(rank):
        return pl.BlockSpec((rank, block), lambda i: (0, i))

    wide = jax.ShapeDtypeStruct((T, mix), f32)
    here = pl.BlockSpec((T, block), lambda i: (0, i))
    return pl.pallas_call(
        functools.partial(recur_kernel, math.gcd(span_most, T)),
        grid=(mix // block,),
        out_shape=[wide, wide, wide, wide, jax.ShapeDtypeStruct((heads, 2 * hc, hc), bf16)],
        in_specs=[
            col(0, block), col(mix, block), col(2 * mix, block),
            fixed(at, grank), fixed(at + grank, drank), fixed(at + grank + drank, rrank),
            weight(grank), weight(drank), weight(rrank),
            pl.BlockSpec((vec.shape[0], block), lambda i: (0, i)),
            here, here,
        ],
        out_specs=[here, here, here, here,
                   pl.BlockSpec((per, 2 * hc, hc), lambda i: (i, 0, 0))],
        compiler_params=pltpu.CompilerParams(vmem_limit_bytes=VMEM_LIMIT),
        cost_estimate=pl.CostEstimate(flops=6 * 10**10, bytes_accessed=10**7, transcendentals=0),
        name="recur",
    )(proj, proj, proj, proj, proj, proj, gw, dw, rw, vec, re, de)


def chain_kernel(n, group, yl_ref, ym_ref, bonus_ref, gate_ref, vec_ref, s0_ref, ms_ref, out_ref,
                 near, whole, far, ns, nr, fs, fr):
    hc = HEAD_CHANNELS
    me = lax.axis_index("sp")
    lo = lax.rem(me, group)
    base = me - lo
    hi = me // group
    groups = n // group
    heads = s0_ref.shape[0]
    near_peer = [base + lax.rem(lo + j, group) for j in range(group)]
    far_peer = [lax.rem(hi + j, groups) * group + lo for j in range(groups)]
    barrier = pltpu.get_barrier_semaphore()
    for peer in near_peer[1:] + far_peer[1:]:
        pl.semaphore_signal(barrier, inc=1, device_id={"sp": peer}, device_id_type=MESH)
    pl.semaphore_wait(barrier, group + groups - 2)
    for j in range(1, group):
        remote(ms_ref, near.at[j], ns.at[j], nr.at[j], near_peer[j]).start()
    near[0] = ms_ref[...]
    for j in range(1, group):
        remote(ms_ref, near.at[j], ns.at[j], nr.at[j], near_peer[j]).wait()
    places = [lax.rem(lo + group - l, group) for l in range(group)]
    current = [near[places[0], h].astype(f32) for h in range(heads)]
    for l in range(1, group):
        step = near[places[l]]
        current = [
            mm2(c, step[h, :hc])
            + jnp.concatenate([jnp.zeros((hc, hc), f32), step[h, hc:].astype(f32)], axis=0)
            for h, c in enumerate(current)
        ]
    for h in range(heads):
        whole[h] = current[h].astype(bf16)
    for j in range(1, groups):
        remote(whole, far.at[j], fs.at[j], fr.at[j], far_peer[j]).start()
    for j in range(1, groups):
        remote(whole, far.at[j], fs.at[j], fr.at[j], far_peer[j]).wait()
    state = [s0_ref[h] for h in range(heads)]

    def advance(state, step, go):
        return [
            jnp.where(go, mm2(s, step[h, :hc]) + step[h, hc:].astype(f32), s)
            for h, s in enumerate(state)
        ]

    for g in range(groups - 1):
        slot = jnp.maximum(lax.rem(hi + groups - g, groups), 1)
        state = advance(state, far[slot], g < hi)
    for l in range(group - 1):
        state = advance(state, near[places[l]], l < lo)
    vec = vec_ref[...]
    parts = []
    for h in range(heads):
        sl = slice(h * hc, (h + 1) * hc)
        reading = yl_ref[:, sl] + mm3(ym_ref[:, sl], state[h], MT)
        center = jnp.mean(reading, axis=1, keepdims=True)
        off = reading - center
        spread = jnp.mean(off * off, axis=1, keepdims=True)
        parts.append(off * lax.rsqrt(spread + 1e-5 * hc))
    headed = halves(parts) * vec[0:1] + vec[1:2] + bonus_ref[...]
    out_ref[...] = (headed * gate_ref[...]).astype(bf16)


def chain(yl, ym, bonus, gate, vec, s0, ms, n, group):
    heads, two, hc = ms.shape
    dma = pltpu.SemaphoreType.DMA
    groups = n // group
    return pl.pallas_call(
        functools.partial(chain_kernel, n, group),
        out_shape=jax.ShapeDtypeStruct(yl.shape, bf16),
        in_specs=[pl.BlockSpec(memory_space=pltpu.VMEM)] * 7,
        out_specs=pl.BlockSpec(memory_space=pltpu.VMEM),
        scratch_shapes=[
            pltpu.VMEM((group, heads, two, hc), bf16),
            pltpu.VMEM((heads, two, hc), bf16),
            pltpu.VMEM((groups, heads, two, hc), bf16),
            dma((group,)), dma((group,)), dma((groups,)), dma((groups,)),
        ],
        compiler_params=pltpu.CompilerParams(
            collective_id=1, has_side_effects=True, vmem_limit_bytes=VMEM_LIMIT
        ),
        cost_estimate=pl.CostEstimate(flops=4 * 10**10, bytes_accessed=10**7, transcendentals=0),
        name="chain",
    )(yl, ym, bonus, gate, vec, s0, ms)


def window_width(scale_index):
    result = jnp.zeros(scale_index.shape, jnp.float32)
    for level, width in enumerate(pool_windows):
        result = jnp.where(scale_index == level, jnp.float32(width), result)
    return result


def window_sums(extended, scale_index, row_total):
    running = jnp.zeros((row_total, extended.shape[1]), jnp.float32)
    chosen = jnp.zeros((row_total, extended.shape[1]), jnp.float32)
    for offset in range(pool_reach):
        running = running + extended[pool_reach - offset : pool_reach - offset + row_total]
        for level, width in enumerate(pool_windows):
            if offset + 1 == width:
                chosen = jnp.where(scale_index[None, :] == level, running, chosen)
    return chosen


def on_device(
    tokens,
    input_norm_scale,
    input_norm_bias,
    query_projection,
    key_projection,
    value_projection,
    pooling_input_projection,
    decay_input_weight,
    rate_input_weight,
    gate_input_weight,
    decay_output_weight,
    rate_output_weight,
    gate_output_weight,
    decay_bias_base,
    learning_rate_base,
    key_prenorm_scale,
    key_learning_scale,
    self_term_weight,
    head_norm_scale,
    head_norm_bias,
    rate_extra_log,
    decay_extra_log,
    starting_head_state,
    pooling_group_matrix,
    pooling_output_scale,
    output_attention_rows,
    output_pooling_rows,
):
    n = lax.axis_size("sp")
    group = math.gcd(n, 4)
    row_total = tokens.shape[0]
    mix_width = query_projection.shape[1]
    out_rows = lax.all_gather(
        jnp.concatenate([output_attention_rows, output_pooling_rows], axis=0), "sp", axis=0
    )
    wide = tokens.astype(f32)
    center = jnp.mean(wide, axis=-1, keepdims=True)
    spread = jnp.mean(jnp.square(wide - center), axis=-1, keepdims=True)
    normed = (
        (wide - center) * lax.rsqrt(spread + 1e-05) * input_norm_scale + input_norm_bias
    ).astype(bf16)
    weights = jnp.concatenate(
        [
            query_projection, key_projection, value_projection, pooling_input_projection,
            gate_input_weight, decay_input_weight, rate_input_weight,
        ],
        axis=1,
    )
    deep, total_cols = weights.shape
    weights = weights.reshape(deep, group, total_cols // group).transpose(1, 0, 2)
    proj = project(normed, weights, n, group)
    pool_in = proj[:, 3 * mix_width:4 * mix_width]
    lows = (gate_input_weight.shape[1], decay_input_weight.shape[1], rate_input_weight.shape[1])
    vec = jnp.stack(
        [decay_bias_base, learning_rate_base, key_prenorm_scale, key_learning_scale,
         self_term_weight, head_norm_scale, head_norm_bias, pooling_output_scale]
    )
    yl, ym, bonus, gate, ms = recur(
        proj, mix_width, lows, gate_output_weight, decay_output_weight, rate_output_weight,
        vec, rate_extra_log, decay_extra_log,
    )
    attn_out = chain(yl, ym, bonus, gate, vec[5:7], starting_head_state, ms, n, group)
    pool_width_dev = pool_in.shape[1]
    groups_dev = pool_width_dev // POOL_GROUP
    previous = passed_along(pool_in[row_total - pool_reach :], "sp", 1)
    extended = jnp.concatenate([previous, pool_in], axis=0).astype(f32)
    group_ids = (
        lax.axis_index("tp") * groups_dev
        + jnp.arange(pool_width_dev, dtype=jnp.int32) // POOL_GROUP
    )
    scale_index = group_ids // (POOL_GROUPS // 4)
    chosen = window_sums(extended, scale_index, row_total)
    position = (lax.axis_index("sp") * row_total + jnp.arange(row_total, dtype=jnp.int32)).astype(
        f32
    )
    counted = jnp.minimum(position[:, None] + 1.0, window_width(scale_index)[None, :])
    pooled = (chosen / counted - pool_in.astype(f32)).astype(bf16)
    pool_out = jnp.concatenate(
        [
            jnp.dot(pooled[:, g * POOL_GROUP:(g + 1) * POOL_GROUP], pooling_group_matrix[g],
                    preferred_element_type=f32)
            for g in range(groups_dev)
        ],
        axis=1,
    )
    pool_out = (pool_out * pooling_output_scale).astype(bf16)
    both = jnp.concatenate([attn_out, pool_out], axis=1)
    mixed = jnp.einsum("tk,skd->tsd", both, out_rows, preferred_element_type=f32)
    mixed = lax.psum_scatter(
        mixed.reshape(row_total, -1).astype(bf16), "tp", scatter_dimension=0, tiled=True
    )
    return mixed.astype(bf16)


def solution(mesh):
    in_specs = (
        P("sp", None),
        P(),
        P(),
        P("sp", "tp"),
        P("sp", "tp"),
        P("sp", "tp"),
        P("sp", "tp"),
        P("sp", None),
        P("sp", None),
        P("sp", None),
        P(None, "tp"),
        P(None, "tp"),
        P(None, "tp"),
        P("tp"),
        P("tp"),
        P("tp"),
        P("tp"),
        P("tp"),
        P("tp"),
        P("tp"),
        P("sp", "tp"),
        P("sp", "tp"),
        P("tp", None, None),
        P("tp", None, None),
        P("tp"),
        P("tp", "sp"),
        P("tp", "sp"),
    )
    out_specs = P(("sp", "tp"), None)
    return jax.shard_map(
        on_device, mesh=mesh, in_specs=in_specs, out_specs=out_specs, check_vma=False
    )
```

time: 711 us -> 207 us (0.29)
  waiting for transfers between devices: 337 us -> 14.6 us
  Pallas kernels: 0 us -> 145 us
  other arithmetic: 139 us -> 6.67 us
  local copies, waits for them, and re-layouts: 93.6 us -> 17.3 us
  blocking collectives: 66.3 us -> 0 us
  matrix products: 51.3 us -> 3.98 us
    all_gather x9 -> x1, waiting for transfers between devices: 322 us -> 0.02 us  [on_device(): lax.all_gather(jnp.concatenate([output_attention_rows, output_pooling_row...]
    pallas_call x0 -> x3, Pallas kernels: none -> 145 us  [the longest x1 96.3 us: project(): pl.pallas_call(functools.partial(project_kernel, n, group), out_shape=jax...]
    another operation x14 -> x1, other arithmetic: 80.9 us -> 0.59 us  [on_device(): jnp.stack([decay_bias_base, learning_rate_base, key_prenorm_scale, key_le...]
    while x46 -> x0, local copies, waits for them, and re-layouts: 72.5 us -> none
    all_gather x2 -> x0, blocking collectives: 66.3 us -> none  [the longest x1 37 us: on_device(): lax.all_gather(decay_input_weight, 'sp', axis=0, tiled=True)]
    dot_general x44 -> x4, matrix products: 47 us -> 0.54 us  [on_device(): jnp.dot(pooled[:, g * POOL_GROUP:(g + 1) * POOL_GROUP], pooling_group_mat...]
    dot_general x2 -> x0, other arithmetic: 25.1 us -> none  [block_recurrence(): jnp.einsum('htk,hsk,htsk->hts', alpha_t, key_t, weight_before, precision=...]
    exp x2 -> x0, other arithmetic: 24.4 us -> none  [block_recurrence(): jnp.exp(jnp.where(upto, total[:, :, None, :] - total[:, None, :, :], -jnp...]
  transfers between devices with their start and end apart: 11 -> 3, of which waited for: 7 -> 1; matrix products, arithmetic and copies ran while one was open for 40% -> 7% of each run, Pallas kernels for 0% -> 71%
where the time goes in v1:
time: 207 us; the launch traced here: 205 us
  Pallas kernels  145 us (70%)
  local copies, waits for them, and re-layouts  17.3 us (8%)
  waiting for transfers between devices  14.6 us (7%)
  between operations  13.7 us (7%)
  other arithmetic  6.67 us (3%)
  starting transfers between devices  4.2 us (2%)
  matrix products  3.98 us (2%)
    pallas_call x1, Pallas kernels, project(): pl.pallas_call(functools.partial(project_kernel, n, group), out_shape=jax...  96.3 us
    pallas_call x1, Pallas kernels, chain(): pl.pallas_call(functools.partial(chain_kernel, n, group), out_shape=jax.S...  37.3 us
    reduce_scatter x1, waiting for transfers between devices, on_device(): lax.psum_scatter(mixed.reshape(row_total, -1).astype(bf16), 'tp', scatter...  14.6 us
    pallas_call x1, Pallas kernels, recur(): pl.pallas_call(functools.partial(recur_kernel, math.gcd(span_most, T)), g...  11.2 us
    unnamed x41, local copies, waits for them, and re-layouts  7.37 us
    all_gather x1, local copies, waits for them, and re-layouts, on_device(): lax.all_gather(jnp.concatenate([output_attention_rows, output_pooling_row...  6.48 us
    ppermute x1, starting transfers between devices, passed_along(): lax.ppermute(value, axis, [(source, source + steps) for source in range(l...  4.16 us
  transfers between devices with their start and end apart: 3, of which 1 were waited for; matrix products, arithmetic and copies ran while one was open for 7% of the time, Pallas kernels for 71%

profile of v1, /device:TPU:11, one launch (start us, length us, event | category | flops | bytes accessed | tf_op | source)
XLA Modules:
  0.0 205.4 jit_solution(7867711149768876001)
XLA Ops:
  6.5 1.7 pad_maximum_fusion
  8.3 0.0 reduce-scatter.2.cloned.1.call-start
  8.4 1.2 convert_reduce_fusion
  9.6 1.3 fusion.2
  10.9 1.0 copy.29
  12.0 1.0 copy.30
  13.0 1.0 copy.31
  14.0 1.0 copy.32
  15.0 1.0 copy.33
  16.0 0.9 copy.34
  16.9 0.9 copy.35
  17.9 1.1 copy.36
  19.0 1.2 fusion.5.normed_ref
  20.3 96.3 %project.1.q_ref.k_ref.v_ref.gl_ref.dl_ref.rl_ref = bf16[128,2560]{1,0:T(8,128)(2,1)} custom-call(bf16[128,2048]{1,0:T(8,128)(2,1)} %fusion.5.normed_ref, bf16[4,128,640]{2,1,0:T(8,128)(2,1)} %bitcast.34), custom_call_target="tpu_custom_call" | custom-call | flops 99999997952 | bytes 10000000 | tf_op jit(solution)/shard_map/project/pallas_call | solution.py:134
  116.5 0.7 slice.81
  117.3 4.2 %collective-permute-start = (bf16[16,512]{1,0:T(8,128)(2,1)S(1)}, bf16[16,512]{1,0:T(8,128)(2,1)S(1)}, u32[]{:S(2)}, u32[]{:S(2)}) collective-permute-start(bf16[16,512]{1,0:T(8,128)(2,1)S(1)} %slice.81), channel_id=1, source_target_pairs={{0,2},{2,4},{4,6},{6,8},{8,10},{10,12},{12,14},{14,16},{16,18},{18... | collective-permute-start | bytes 49160 | tf_op jit(solution)/shard_map/ppermute | solution.py:52
  121.5 0.6 stack.37.vec_ref
  122.1 11.2 %recur.1 = (f32[128,512]{1,0:T(8,128)}, f32[128,512]{1,0:T(8,128)}, f32[128,512]{1,0:T(8,128)}, f32[128,512]{1,0:T(8,128)}, bf16[8,128,64]{2,1,0:T(8,128)(2,1)}) custom-call(bf16[128,2560]{1,0:T(8,128)(2,1)} %project.1.q_ref.k_ref.v_ref.gl_ref.dl_ref.rl_ref, bf16[128,2560]{1,0:T(8,128)(2,1)} %project.1.q_ref.k_ref.v_ref.gl_ref.dl_ref.rl_ref, ...), custom_call_target="tpu_custom_call" | custom-call | flops 60000002048 | bytes 10000000 | tf_op jit(solution)/shard_map/recur/pallas_call | solution.py:289
  133.4 0.6 pad_maximum_fusion.1.vec_ref
  134.0 37.3 %chain.1 = bf16[128,512]{1,0:T(8,128)(2,1)} custom-call(f32[128,512]{1,0:T(8,128)} %get-tuple-element.10.yl_ref, f32[128,512]{1,0:T(8,128)} %get-tuple-element.11.ym_ref, f32[128,512]{1,0:T(8,128)} %get-tuple-element.12.bonus_ref, f32[128,512]{1,0:T(8,128)} %get-tuple-element.13.gate_ref, f32[2,512]{1,0:T(2,128)} %pad_maximum_fusion.1.vec_ref, ...), custom_call_target="tpu_custom_call" | custom-call | flops 40000000000 | bytes 10000000 | tf_op jit(solution)/shard_map/chain/pallas_call | solution.py:373
  171.5 0.4 fusion.14
  171.9 0.4 copy-done.3
  172.3 0.1 fusion.15
  172.4 0.1 fusion.17
  172.6 0.1 fusion.19
  172.7 0.1 fusion.21
  172.9 0.0 all-gather.3.cloned.1.call-done
  172.9 6.5 %copy.37 = bf16[16,1024,128]{1,2,0:T(8,128)(2,1)} copy(bf16[16,1024,128]{2,1,0:T(8,128)(2,1)} %bitcast.30) | data formatting | bytes 8388608 | tf_op jit(solution)/shard_map/all_gather | solution.py:443
  179.4 3.4 %fusion.10 = f32[128,2048]{0,1:S(1)} fusion(bf16[1024,2048]{0,1:T(8,128)(2,1)} %bitcast.29, bf16[128,512]{1,0:T(8,128)(2,1)S(1)} %fusion.9, bf16[128,512]{1,0:T(8,128)(2,1)S(1)} %copy-done.2), kind=kOutput, calls=%fused_computation.28 | convolution fusion | flops 537395200 | bytes 5505024
  182.9 0.1 convert_element_type.38
  183.0 1.0 copy.38
  184.0 14.6 %reduce-scatter.2.cloned.1.call-done = bf16[64,2048]{1,0:T(8,128)(2,1)} async-done(((bf16[128,2048]{1,0:T(8,128)(2,1)}), bf16[64,2048]{1,0:T(8,128)(2,1)}) %reduce-scatter.2.cloned.1.call-update) | async-done | bytes 262160 | tf_op jit(solution)/shard_map/reduce_scatter | solution.py:499
  (48 shorter events, 0.3 us)
Async XLA Ops:
  6.5 12.5 %copy-start = (bf16[128,2048]{1,0:T(8,128)(2,1)S(1)}, bf16[128,2048]{1,0:T(8,128)(2,1)}, u32[]{:S(2)}) copy-start(bf16[128,2048]{1,0:T(8,128)(2,1)} %param.27) | copy-start | bytes 1572868
  6.5 12.5 %copy-start.4 = (f32[2048]{0:T(1024)S(1)}, f32[2048]{0:T(1024)}, u32[]{:S(2)}) copy-start(f32[2048]{0:T(1024)} %param.29) | copy-start | bytes 24580
  6.5 12.5 %copy-start.5 = (f32[2048]{0:T(1024)S(1)}, f32[2048]{0:T(1024)}, u32[]{:S(2)}) copy-start(f32[2048]{0:T(1024)} %param.28) | copy-start | bytes 24580
  6.5 166.4 %all-gather.3.cloned.1.call-start = ((), (), s32[]{:S(2)}) async-start(), calls=%async_computation.2 | async-start | bytes 4456448 | tf_op jit(solution)/shard_map/all_gather | solution.py:443
  8.3 190.3 %reduce-scatter.2.cloned.1.call-start = ((), (), s32[]{:S(2)}) async-start(), calls=%async_computation.1 | async-start | bytes 786432 | tf_op jit(solution)/shard_map/reduce_scatter | solution.py:499
  20.2 101.2 %copy-start.6 = (f32[512]{0:T(512)S(1)}, f32[512]{0:T(512)}, u32[]{:S(2)}) copy-start(f32[512]{0:T(512)} %param.51) | copy-start | bytes 6148
  20.2 101.2 %copy-start.7 = (f32[512]{0:T(512)S(1)}, f32[512]{0:T(512)}, u32[]{:S(2)}) copy-start(f32[512]{0:T(512)} %param.45) | copy-start | bytes 6148
  20.2 101.2 %copy-start.8 = (f32[512]{0:T(512)S(1)}, f32[512]{0:T(512)}, u32[]{:S(2)}) copy-start(f32[512]{0:T(512)} %param.46) | copy-start | bytes 6148
  20.2 101.2 %copy-start.9 = (f32[512]{0:T(512)S(1)}, f32[512]{0:T(512)}, u32[]{:S(2)}) copy-start(f32[512]{0:T(512)} %param.40) | copy-start | bytes 6148
  20.2 101.2 %copy-start.10 = (f32[512]{0:T(512)S(1)}, f32[512]{0:T(512)}, u32[]{:S(2)}) copy-start(f32[512]{0:T(512)} %param.41) | copy-start | bytes 6148
  20.2 101.2 %copy-start.11 = (f32[512]{0:T(512)S(1)}, f32[512]{0:T(512)}, u32[]{:S(2)}) copy-start(f32[512]{0:T(512)} %param.42) | copy-start | bytes 6148
  20.2 101.2 %copy-start.12 = (f32[512]{0:T(512)S(1)}, f32[512]{0:T(512)}, u32[]{:S(2)}) copy-start(f32[512]{0:T(512)} %param.43) | copy-start | bytes 6148
  20.3 101.2 %copy-start.13 = (f32[512]{0:T(512)S(1)}, f32[512]{0:T(512)}, u32[]{:S(2)}) copy-start(f32[512]{0:T(512)} %param.44) | copy-start | bytes 6148
  117.3 54.2 %collective-permute-start = (bf16[16,512]{1,0:T(8,128)(2,1)S(1)}, bf16[16,512]{1,0:T(8,128)(2,1)S(1)}, u32[]{:S(2)}, u32[]{:S(2)}) collective-permute-start(bf16[16,512]{1,0:T(8,128)(2,1)S(1)} %slice.81), channel_id=1, source_target_pairs={{0,2},{2,4},{4,6},{6,8},{8,10},{10,12},{12,14},{14,16},{16,18},{18... | collective-permute-start | bytes 49160 | tf_op jit(solution)/shard_map/ppermute | solution.py:52
  134.0 37.4 %slice-start = ((bf16[128,2560]{1,0:T(8,128)(2,1)}), bf16[128,512]{1,0:T(8,128)(2,1)S(1)}, s32[]{:S(2)}) async-start(bf16[128,2560]{1,0:T(8,128)(2,1)} %project.1.q_ref.k_ref.v_ref.gl_ref.dl_ref.rl_ref), calls=%async_computation.3 | async-start | bytes 262144 | tf_op jit(solution)/shard_map/slice | solution.py:462
  134.0 37.4 %copy-start.1 = (bf16[128,2560]{1,0:T(8,128)(2,1)S(1)}, bf16[128,2560]{1,0:T(8,128)(2,1)}, u32[]{:S(2)}) copy-start(bf16[128,2560]{1,0:T(8,128)(2,1)} %project.1.q_ref.k_ref.v_ref.gl_ref.dl_ref.rl_ref) | copy-start | bytes 1966084
  171.4 0.9 copy-start.3
  172.9 6.5 %copy-start.2 = (bf16[128,512]{1,0:T(8,128)(2,1)S(1)}, bf16[128,512]{1,0:T(8,128)(2,1)}, u32[]{:S(2)}) copy-start(bf16[128,512]{1,0:T(8,128)(2,1)} %chain.1) | copy-start | bytes 393220
Sparse Core Ops, SparseCore 0:
  10.1 128.0 all-gather.2
  184.1 14.4 reduce-scatter.1

commit v2 on v1

--- a/solution.py
+++ b/solution.py
@@ -59,97 +59,211 @@
     )
 
 
-def project_kernel(n, group, normed_ref, w_ref, out_ref, nall, wall, res, got,
-                   own_sem, ns, nr, ws, wr, rs, rr):
+def project_kernel(n, group, pieces, tok_ref, norm_ref, *args):
+    mats = args[:7]
+    (oa_ref, op_ref, out_ref, ow_ref, wown, nall, wall, res, got, asm_sem, own_sem,
+     ns, nr, ws, wr, us, ur, ds, dr, rs, rr, oas, oar, ops, opr) = args[7:]
     me = lax.axis_index("sp")
     lo = lax.rem(me, group)
     base = me - lo
-    rows = normed_ref.shape[0]
-    deep = w_ref.shape[1]
-    wide = w_ref.shape[2]
-    barrier = pltpu.get_barrier_semaphore()
-    for j in range(1, n):
-        pl.semaphore_signal(barrier, inc=1, device_id={"sp": lax.rem(me + j, n)}, device_id_type=MESH)
-    pl.semaphore_wait(barrier, n - 1)
+    hi = me // group
+    groups = n // group
+    rows = tok_ref.shape[0]
+    deep, wide = wown.shape[1:]
+    mix = oa_ref.shape[0]
+    near_peer = [base + lax.rem(lo + j, group) for j in range(group)]
+    far_at = [lax.rem(hi + j, groups) for j in range(groups)]
+    far_peer = [at * group + lo for at in far_at]
 
     def row_slot(index, size):
         return pl.ds(pl.multiple_of(index * size, size), size)
 
+    assemble = []
+    for i, (mat, source, quarter, target, width) in enumerate(pieces):
+        c = pltpu.make_async_copy(
+            mats[mat].at[:, source:source + width],
+            wown.at[quarter, :, target:target + width], asm_sem.at[i],
+        )
+        c.start()
+        assemble.append(c)
+    own_out = (
+        pltpu.make_async_copy(oa_ref, ow_ref.at[hi, :mix], own_sem.at[2]),
+        pltpu.make_async_copy(op_ref, ow_ref.at[hi, mix:], own_sem.at[3]),
+    )
+    for c in own_out:
+        c.start()
+    barrier = pltpu.get_barrier_semaphore()
+    for peer in near_peer[1:] + far_peer[1:]:
+        pl.semaphore_signal(barrier, inc=1, device_id={"sp": peer}, device_id_type=MESH)
+    for c in assemble:
+        c.wait()
+    pl.semaphore_wait(barrier, group + groups - 2)
+
     def w_copy(j):
-        peer = lax.rem(me + j, n)
-        return remote(w_ref.at[lax.rem(peer, group)], wall.at[row_slot(me, deep)],
-                      ws.at[j], wr.at[j], peer)
+        return remote(wown.at[lax.rem(lo + j, group)], wall.at[row_slot(me, deep)],
+                      ws.at[j], wr.at[j], near_peer[j])
 
     def w_land(j):
-        source = lax.rem(me + n - j, n)
-        return remote(w_ref.at[0], wall.at[row_slot(source, deep)], ws.at[j], wr.at[j], source)
+        source = base + lax.rem(lo + group - j, group)
+        return remote(wown.at[0], wall.at[row_slot(source, deep)], ws.at[j], wr.at[j], source)
 
     def n_copy(j):
-        return remote(normed_ref, nall.at[row_slot(lo, rows)], ns.at[j], nr.at[j],
-                      base + lax.rem(lo + j, group))
+        return remote(nall.at[row_slot(lo, rows)], nall.at[row_slot(lo, rows)], ns.at[j], nr.at[j],
+                      near_peer[j])
 
     def n_land(j):
         at = lax.rem(lo + group - j, group)
-        return remote(normed_ref, nall.at[row_slot(at, rows)], ns.at[j], nr.at[j], base + at)
-
+        slot = nall.at[row_slot(at, rows)]
+        return remote(slot, slot, ns.at[j], nr.at[j], base + at)
+
+    def block(index):
+        return wall.at[row_slot(index, group * deep)]
+
+    for j in range(1, group):
+        w_copy(j).start()
+    own_w = pltpu.make_async_copy(wown.at[lo], wall.at[row_slot(me, deep)], own_sem.at[1])
+    own_w.start()
+    x = tok_ref[...].astype(f32)
+    off = x - jnp.mean(x, axis=1, keepdims=True)
+    spread = jnp.mean(off * off, axis=1, keepdims=True)
+    nall[row_slot(lo, rows), :] = (
+        off * lax.rsqrt(spread + 1e-5) * norm_ref[0:1] + norm_ref[1:2]
+    ).astype(bf16)
     for j in range(1, group):
         n_copy(j).start()
-    for j in range(1, n):
-        w_copy(j).start()
-    own = (
-        pltpu.make_async_copy(normed_ref, nall.at[row_slot(lo, rows)], own_sem.at[0]),
-        pltpu.make_async_copy(w_ref.at[lo], wall.at[row_slot(me, deep)], own_sem.at[1]),
-    )
-    for c in own:
-        c.start()
-    for c in own:
-        c.wait()
+    own_w.wait()
+    for j in range(1, group):
+        w_land(j).wait_recv()
+
+    def up(s):
+        return remote(block(hi - s), block(hi - s), us.at[s], ur.at[s], me + group)
+
+    def up_land(s):
+        return remote(block(hi - 1 - s), block(hi - 1 - s), us.at[s], ur.at[s], me - group)
+
+    def down(s):
+        return remote(block(hi + s), block(hi + s), ds.at[s], dr.at[s], me - group)
+
+    def down_land(s):
+        return remote(block(hi + 1 + s), block(hi + 1 + s), ds.at[s], dr.at[s], me + group)
+
+    def landed(s):
+        @pl.when(hi - 1 - s >= 0)
+        def _():
+            up_land(s).wait_recv()
+
+        @pl.when(hi + 1 + s < groups)
+        def _():
+            down_land(s).wait_recv()
+
+    def sends(s, act):
+        @pl.when((hi - s >= 0) & (hi + 1 < groups))
+        def _():
+            act(up(s))
+
+        @pl.when((hi + s < groups) & (hi >= 1))
+        def _():
+            act(down(s))
+
+    for s in range(groups - 1):
+        if s > 0:
+            landed(s - 1)
+        sends(s, lambda c: c.start())
+
+    def o_copies(j):
+        return (
+            remote(oa_ref, ow_ref.at[hi, :mix], oas.at[j], oar.at[j], far_peer[j]),
+            remote(op_ref, ow_ref.at[hi, mix:], ops.at[j], opr.at[j], far_peer[j]),
+        )
+
+    def o_lands(j):
+        at = lax.rem(hi + groups - j, groups)
+        return (
+            remote(oa_ref, ow_ref.at[at, :mix], oas.at[j], oar.at[j], at * group + lo),
+            remote(op_ref, ow_ref.at[at, mix:], ops.at[j], opr.at[j], at * group + lo),
+        )
+
+    for j in range(1, groups):
+        for c in o_copies(j):
+            c.start()
     for j in range(1, group):
         n_land(j).wait_recv()
-    for j in range(1, n):
-        w_land(j).wait_recv()
+    if groups > 1:
+        landed(groups - 2)
     weights = wall[...]
+
+    def r_copy(j):
+        return remote(res.at[j], got.at[j], rs.at[j], rr.at[j], near_peer[j])
+
     for j in range(1, group):
         at = lax.rem(lo + j, group)
         part = jnp.dot(nall[row_slot(at, rows), :], weights, preferred_element_type=f32)
         res[j] = part.astype(bf16)
-        remote(res.at[j], got.at[j], rs.at[j], rr.at[j], base + at).start()
-    got[0] = jnp.dot(normed_ref[...], weights, preferred_element_type=f32).astype(bf16)
+        r_copy(j).start()
+    got[0] = jnp.dot(
+        nall[row_slot(lo, rows), :], weights, preferred_element_type=f32
+    ).astype(bf16)
     for j in range(1, group):
         n_copy(j).wait_send()
-    for j in range(1, n):
         w_copy(j).wait_send()
-    for j in range(1, group):
-        c = remote(res.at[j], got.at[j], rs.at[j], rr.at[j], base + lax.rem(lo + j, group))
-        c.wait_send()
-        c.wait_recv()
+    for s in range(groups - 1):
+        sends(s, lambda c: c.wait_send())
+    for j in range(1, group):
+        r_copy(j).wait_send()
+        r_copy(j).wait_recv()
     for col in range(group):
         out_ref[:, col * wide:(col + 1) * wide] = got[lax.rem(lo + group - col, group)]
-
-
-def project(normed, weights, n, group):
-    rows, width = normed.shape
-    _, deep, wide = weights.shape
+    for c in own_out:
+        c.wait()
+    for j in range(1, groups):
+        for c in o_copies(j):
+            c.wait_send()
+        for c in o_lands(j):
+            c.wait_recv()
+
+
+def project(tokens, norm, mats, out_attn, out_pool, n, group):
+    rows, width = tokens.shape
+    deep = mats[0].shape[0]
+    total = sum(m.shape[1] for m in mats)
+    wide = total // group
+    groups = n // group
+    mix, cpc = out_attn.shape
+    pool = out_pool.shape[0]
+    pieces = []
+    start = 0
+    for i, m in enumerate(mats):
+        done = 0
+        while done < m.shape[1]:
+            place = start + done
+            size = min(m.shape[1] - done, wide - place % wide)
+            pieces.append((i, done, place // wide, place % wide, size))
+            done += size
+        start += m.shape[1]
     dma = pltpu.SemaphoreType.DMA
+    vm = pl.BlockSpec(memory_space=pltpu.VMEM)
     return pl.pallas_call(
-        functools.partial(project_kernel, n, group),
-        out_shape=jax.ShapeDtypeStruct((rows, group * wide), bf16),
-        in_specs=[pl.BlockSpec(memory_space=pltpu.VMEM)] * 2,
-        out_specs=pl.BlockSpec(memory_space=pltpu.VMEM),
+        functools.partial(project_kernel, n, group, tuple(pieces)),
+        out_shape=[
+            jax.ShapeDtypeStruct((rows, group * wide), bf16),
+            jax.ShapeDtypeStruct((groups, mix + pool, cpc), bf16),
+        ],
+        in_specs=[vm, vm] + [pl.BlockSpec(memory_space=pl.ANY)] * len(mats) + [vm, vm],
+        out_specs=[vm, vm],
         scratch_shapes=[
+            pltpu.VMEM((group, deep, wide), bf16),
             pltpu.VMEM((group * rows, width), bf16),
             pltpu.VMEM((n * deep, wide), bf16),
             pltpu.VMEM((group, rows, wide), bf16),
             pltpu.VMEM((group, rows, wide), bf16),
-            dma((2,)),
-            dma((group,)), dma((group,)), dma((n,)), dma((n,)), dma((group,)), dma((group,)),
-        ],
+            dma((len(pieces),)), dma((4,)),
+        ] + [dma((group,))] * 4 + [dma((groups,))] * 4 + [dma((group,))] * 2 + [dma((groups,))] * 4,
         compiler_params=pltpu.CompilerParams(
             collective_id=0, has_side_effects=True, vmem_limit_bytes=VMEM_LIMIT
         ),
         cost_estimate=pl.CostEstimate(flops=10**11, bytes_accessed=10**7, transcendentals=0),
         name="project",
-    )(normed, weights)
+    )(tokens, norm, *mats, out_attn, out_pool)
 
 
 def halves(parts):
@@ -305,8 +419,9 @@
     )(proj, proj, proj, proj, proj, proj, gw, dw, rw, vec, re, de)
 
 
-def chain_kernel(n, group, yl_ref, ym_ref, bonus_ref, gate_ref, vec_ref, s0_ref, ms_ref, out_ref,
-                 near, whole, far, ns, nr, fs, fr):
+def chain_kernel(n, group, m, yl_ref, ym_ref, bonus_ref, gate_ref, vec_ref, s0_ref, ms_ref,
+                 pool_ref, ow_ref, out_ref, near, whole, far, attn, act_a, act_p, res, got,
+                 ns, nr, fs, fr, as_, ar, ps, pr, rs, rr):
     hc = HEAD_CHANNELS
     me = lax.axis_index("sp")
     lo = lax.rem(me, group)
@@ -314,14 +429,29 @@
     hi = me // group
     groups = n // group
     heads = s0_ref.shape[0]
+    tp = lax.axis_index("tp")
+    mix = attn.shape[1]
+    rt, cpc = out_ref.shape[0], ow_ref.shape[2]
     near_peer = [base + lax.rem(lo + j, group) for j in range(group)]
     far_peer = [lax.rem(hi + j, groups) * group + lo for j in range(groups)]
     barrier = pltpu.get_barrier_semaphore()
-    for peer in near_peer[1:] + far_peer[1:]:
-        pl.semaphore_signal(barrier, inc=1, device_id={"sp": peer}, device_id_type=MESH)
-    pl.semaphore_wait(barrier, group + groups - 2)
+    tp_at = [lax.rem(tp + d, m) for d in range(m)]
+    for j in range(group):
+        for d in range(m):
+            if j + d > 0:
+                pl.semaphore_signal(barrier, inc=1, device_id={"sp": near_peer[j], "tp": tp_at[d]},
+                                    device_id_type=MESH)
+    for peer in far_peer[1:]:
+        pl.semaphore_signal(barrier, inc=1, device_id={"sp": peer, "tp": tp}, device_id_type=MESH)
+    pl.semaphore_wait(barrier, group * m + groups - 2)
     for j in range(1, group):
         remote(ms_ref, near.at[j], ns.at[j], nr.at[j], near_peer[j]).start()
+    def p_copy(j):
+        return remote(pool_ref, act_p.at[j], ps.at[j], pr.at[j], near_peer[j])
+
+    for j in range(1, group):
+        p_copy(j).start()
+    act_p[0] = pool_ref[...]
     near[0] = ms_ref[...]
     for j in range(1, group):
         remote(ms_ref, near.at[j], ns.at[j], nr.at[j], near_peer[j]).wait()
@@ -363,30 +493,83 @@
         spread = jnp.mean(off * off, axis=1, keepdims=True)
         parts.append(off * lax.rsqrt(spread + 1e-5 * hc))
     headed = halves(parts) * vec[0:1] + vec[1:2] + bonus_ref[...]
-    out_ref[...] = (headed * gate_ref[...]).astype(bf16)
-
-
-def chain(yl, ym, bonus, gate, vec, s0, ms, n, group):
+    attn[...] = (headed * gate_ref[...]).astype(bf16)
+
+    def a_copy(j):
+        return remote(attn, act_a.at[j], as_.at[j], ar.at[j], near_peer[j])
+
+    def r_copy(j, d):
+        owner = base + lax.rem(lo + group - j, group)
+        return pltpu.make_async_remote_copy(
+            src_ref=res.at[j, tp_at[d]], dst_ref=got.at[j, d],
+            send_sem=rs.at[j * m + d], recv_sem=rr.at[j * m + d],
+            device_id={"sp": owner, "tp": tp_at[d]}, device_id_type=MESH,
+        )
+
+    for j in range(1, group):
+        a_copy(j).start()
+    for j in range(group):
+        if j > 0:
+            p_copy(j).wait()
+            a_copy(j).wait()
+        left = attn[...] if j == 0 else act_a[j]
+        pooled = act_p[j]
+        for g in range(groups):
+            part = (
+                jnp.dot(left, ow_ref[g, :mix], preferred_element_type=f32)
+                + jnp.dot(pooled, ow_ref[g, mix:], preferred_element_type=f32)
+            ).astype(bf16)
+            for t in range(m):
+                res[j, t, g] = part[t * rt:(t + 1) * rt]
+        for d in range(m):
+            if j + d > 0:
+                r_copy(j, d).start()
+    got[0, 0] = res[0, tp]
+    for j in range(group):
+        for d in range(m):
+            if j + d > 0:
+                r_copy(j, d).wait()
+    for place in range(group):
+        j = lax.rem(place + group - lo, group)
+        total = got[j, 0].astype(f32)
+        for d in range(1, m):
+            total = total + got[j, d].astype(f32)
+        total = total.astype(bf16)
+        for g in range(groups):
+            at = (g * group + place) * cpc
+            out_ref[:, at:at + cpc] = total[g]
+
+
+def chain(yl, ym, bonus, gate, vec, s0, ms, pool_out, out_rows, n, group, m):
+    T, mix = yl.shape
+    cpc = out_rows.shape[2]
     heads, two, hc = ms.shape
     dma = pltpu.SemaphoreType.DMA
     groups = n // group
     return pl.pallas_call(
-        functools.partial(chain_kernel, n, group),
-        out_shape=jax.ShapeDtypeStruct(yl.shape, bf16),
-        in_specs=[pl.BlockSpec(memory_space=pltpu.VMEM)] * 7,
+        functools.partial(chain_kernel, n, group, m),
+        out_shape=jax.ShapeDtypeStruct((T // m, n * cpc), bf16),
+        in_specs=[pl.BlockSpec(memory_space=pltpu.VMEM)] * 9,
         out_specs=pl.BlockSpec(memory_space=pltpu.VMEM),
         scratch_shapes=[
             pltpu.VMEM((group, heads, two, hc), bf16),
             pltpu.VMEM((heads, two, hc), bf16),
             pltpu.VMEM((groups, heads, two, hc), bf16),
+            pltpu.VMEM((T, mix), bf16),
+            pltpu.VMEM((group, T, mix), bf16),
+            pltpu.VMEM((group,) + pool_out.shape, bf16),
+            pltpu.VMEM((group, m, groups, T // m, cpc), bf16),
+            pltpu.VMEM((group, m, groups, T // m, cpc), bf16),
             dma((group,)), dma((group,)), dma((groups,)), dma((groups,)),
+            dma((group,)), dma((group,)), dma((group,)), dma((group,)),
+            dma((group * m,)), dma((group * m,)),
         ],
         compiler_params=pltpu.CompilerParams(
             collective_id=1, has_side_effects=True, vmem_limit_bytes=VMEM_LIMIT
         ),
         cost_estimate=pl.CostEstimate(flops=4 * 10**10, bytes_accessed=10**7, transcendentals=0),
         name="chain",
-    )(yl, ym, bonus, gate, vec, s0, ms)
+    )(yl, ym, bonus, gate, vec, s0, ms, pool_out, out_rows)
 
 
 def window_width(scale_index):
@@ -440,25 +623,14 @@
     group = math.gcd(n, 4)
     row_total = tokens.shape[0]
     mix_width = query_projection.shape[1]
-    out_rows = lax.all_gather(
-        jnp.concatenate([output_attention_rows, output_pooling_rows], axis=0), "sp", axis=0
-    )
-    wide = tokens.astype(f32)
-    center = jnp.mean(wide, axis=-1, keepdims=True)
-    spread = jnp.mean(jnp.square(wide - center), axis=-1, keepdims=True)
-    normed = (
-        (wide - center) * lax.rsqrt(spread + 1e-05) * input_norm_scale + input_norm_bias
-    ).astype(bf16)
-    weights = jnp.concatenate(
-        [
-            query_projection, key_projection, value_projection, pooling_input_projection,
-            gate_input_weight, decay_input_weight, rate_input_weight,
-        ],
-        axis=1,
-    )
-    deep, total_cols = weights.shape
-    weights = weights.reshape(deep, group, total_cols // group).transpose(1, 0, 2)
-    proj = project(normed, weights, n, group)
+    mats = (
+        query_projection, key_projection, value_projection, pooling_input_projection,
+        gate_input_weight, decay_input_weight, rate_input_weight,
+    )
+    proj, out_rows = project(
+        tokens, jnp.stack([input_norm_scale, input_norm_bias]), mats,
+        output_attention_rows, output_pooling_rows, n, group,
+    )
     pool_in = proj[:, 3 * mix_width:4 * mix_width]
     lows = (gate_input_weight.shape[1], decay_input_weight.shape[1], rate_input_weight.shape[1])
     vec = jnp.stack(
@@ -469,7 +641,6 @@
         proj, mix_width, lows, gate_output_weight, decay_output_weight, rate_output_weight,
         vec, rate_extra_log, decay_extra_log,
     )
-    attn_out = chain(yl, ym, bonus, gate, vec[5:7], starting_head_state, ms, n, group)
     pool_width_dev = pool_in.shape[1]
     groups_dev = pool_width_dev // POOL_GROUP
     previous = passed_along(pool_in[row_total - pool_reach :], "sp", 1)
@@ -494,12 +665,10 @@
         axis=1,
     )
     pool_out = (pool_out * pooling_output_scale).astype(bf16)
-    both = jnp.concatenate([attn_out, pool_out], axis=1)
-    mixed = jnp.einsum("tk,skd->tsd", both, out_rows, preferred_element_type=f32)
-    mixed = lax.psum_scatter(
-        mixed.reshape(row_total, -1).astype(bf16), "tp", scatter_dimension=0, tiled=True
-    )
-    return mixed.astype(bf16)
+    return chain(
+        yl, ym, bonus, gate, vec[5:7], starting_head_state, ms, pool_out, out_rows,
+        n, group, lax.axis_size("tp"),
+    )
 
 
 def solution(mesh):

time: 207 us -> 164 us (0.79)
  waiting for transfers between devices: 14.6 us -> 0.01 us
  between operations: 13.7 us -> 0.15 us
  local copies, waits for them, and re-layouts: 17.3 us -> 5.31 us
  matrix products: 3.98 us -> 0.54 us
  Pallas kernels: 145 us -> 148 us
  other arithmetic: 6.67 us -> 4.02 us
    reduce_scatter x1 -> x0, waiting for transfers between devices: 14.6 us -> none  [on_device(): lax.psum_scatter(mixed.reshape(row_total, -1).astype(bf16), 'tp', scatter...]
    all_gather x1 -> x0, local copies, waits for them, and re-layouts: 6.48 us -> none  [on_device(): lax.all_gather(jnp.concatenate([output_attention_rows, output_pooling_row...]
    unnamed x41 -> x19, local copies, waits for them, and re-layouts: 7.37 us -> 3.04 us
    unnamed x1 -> x0, matrix products: 3.45 us -> none
    pallas_call x2, Pallas kernels: 134 us -> 136 us  [the longest x1 69.5 us: project(): pl.pallas_call(functools.partial(project_kernel, n, group, tuple(pieces))...]
    reduce_sum x2 -> x0, other arithmetic: 2.53 us -> none  [the longest x1 1.33 us: on_device(): spread = jnp.mean(jnp.square(wide - center), axis=-1, keepdims=True)]
  transfers between devices with their start and end apart: 3 -> 1, of which waited for: 1 -> 0; matrix products, arithmetic and copies ran while one was open for 7% -> 1% of each run, Pallas kernels for 71% -> 7%
where the time goes in v2:
time: 164 us
  Pallas kernels  148 us (90%)
  starting transfers between devices  5.88 us (4%)
  local copies, waits for them, and re-layouts  5.31 us (3%)
  other arithmetic  4.02 us (2%)
    pallas_call x1, Pallas kernels, project(): pl.pallas_call(functools.partial(project_kernel, n, group, tuple(pieces))...  69.5 us
    pallas_call x1, Pallas kernels, chain(): pl.pallas_call(functools.partial(chain_kernel, n, group, m), out_shape=ja...  67 us
    pallas_call x1, Pallas kernels, recur(): pl.pallas_call(functools.partial(recur_kernel, math.gcd(span_most, T)), g...  11.2 us
    ppermute x1, starting transfers between devices, passed_along(): lax.ppermute(value, axis, [(source, source + steps) for source in range(l...  5.88 us
  transfers between devices with their start and end apart: 1, of which 0 were waited for; matrix products, arithmetic and copies ran while one was open for 1% of the time, Pallas kernels for 7%

profile of v2, /device:TPU:11, one launch (start us, length us, event | category | flops | bytes accessed | tf_op | source)
XLA Modules:
  0.0 163.6 jit_solution(5644845971539500204)
XLA Ops:
  0.0 1.3 pad_maximum_fusion.norm_ref
  1.3 0.0 copy-start.5
  1.3 0.0 copy-start.6
  1.3 0.0 copy-start.7
  1.4 69.5 %project.1 = (bf16[128,2560]{1,0:T(8,128)(2,1)}, bf16[4,1024,128]{2,1,0:T(8,128)(2,1)}) custom-call(bf16[128,2048]{1,0:T(8,128)(2,1)} %tok_ref.1, f32[2,2048]{1,0:T(2,128)} %pad_maximum_fusion.norm_ref, bf16[128,512]{1,0:T(8,128)(2,1)} %args_0_.4, bf16[128,512]{1,0:T(8,128)(2,1)} %args_1_.4, bf16[128,512]{1,0:T(8,128)(2,1)} %args_2_.4, ...), custom_call_target="tpu_custom_call" | custom-call | flops 99999997952 | bytes 10000000 | tf_op jit(solution)/shard_map/project/pallas_call | solution.py:245
  70.8 0.7 slice.81
  71.5 5.9 %collective-permute-start = (bf16[16,512]{1,0:T(8,128)(2,1)S(1)}, bf16[16,512]{1,0:T(8,128)(2,1)S(1)}, u32[]{:S(2)}, u32[]{:S(2)}) collective-permute-start(bf16[16,512]{1,0:T(8,128)(2,1)S(1)} %slice.81), channel_id=1, source_target_pairs={{0,2},{2,4},{4,6},{6,8},{8,10},{10,12},{12,14},{14,16},{16,18},{18... | collective-permute-start | bytes 49160 | tf_op jit(solution)/shard_map/ppermute | solution.py:52
  77.5 0.0 copy-start.3
  77.5 0.0 copy-start.2
  77.5 0.7 copy-done.3
  78.2 0.0 copy-done.2
  78.2 0.6 pad_maximum_fusion.1.vec_ref
  78.8 0.0 copy-done.5
  78.8 0.0 copy-done.6
  78.8 0.0 copy-done.7
  78.8 0.0 copy-done.8
  78.8 0.6 copy-done.4
  79.5 0.0 copy-done.1
  79.5 0.6 stack.49.vec_ref
  80.1 11.2 %recur.1 = (f32[128,512]{1,0:T(8,128)}, f32[128,512]{1,0:T(8,128)}, f32[128,512]{1,0:T(8,128)}, f32[128,512]{1,0:T(8,128)}, bf16[8,128,64]{2,1,0:T(8,128)(2,1)}) custom-call(bf16[128,2560]{1,0:T(8,128)(2,1)} %get-tuple-element.12.q_ref.k_ref.v_ref.gl_ref.dl_ref.rl_ref, bf16[128,2560]{1,0:T(8,128)(2,1)} %get-tuple-element.12.q_ref.k_ref.v_ref.gl_ref.dl_ref.rl_ref, ...), custom_call_target="tpu_custom_call" | custom-call | flops 60000002048 | bytes 10000000 | tf_op jit(solution)/shard_map/recur/pallas_call | solution.py:403
  91.3 0.9 slice.82
  92.2 0.0 collective-permute-done
  92.3 0.0 copy-start
  92.3 1.3 fusion.4
  93.6 0.0 copy-done
  93.6 0.1 fusion.11
  93.8 0.1 fusion.5
  93.9 0.1 fusion.7
  94.0 0.1 fusion.9
  94.2 0.7 fusion.3.pool_ref
  94.9 67.0 %chain.1 = bf16[64,2048]{1,0:T(8,128)(2,1)} custom-call(f32[128,512]{1,0:T(8,128)} %get-tuple-element.13.yl_ref, f32[128,512]{1,0:T(8,128)} %get-tuple-element.14.ym_ref, f32[128,512]{1,0:T(8,128)} %get-tuple-element.15.bonus_ref, f32[128,512]{1,0:T(8,128)} %get-tuple-element.16.gate_ref, f32[2,512]{1,0:T(2,128)} %pad_maximum_fusion.1.vec_ref, ...), custom_call_target="tpu_custom_call" | custom-call | flops 40000000000 | bytes 10000000 | tf_op jit(solution)/shard_map/chain/pallas_call | solution.py:549
  161.9 1.7 %copy.37 = bf16[64,2048]{1,0:T(8,128)(2,1)} copy(bf16[64,2048]{1,0:T(8,128)(2,1)} %chain.1) | data formatting | bytes 524288
  (8 shorter events, 0.1 us)
Async XLA Ops:
  1.3 77.5 %copy-start.5 = (f32[512]{0:T(512)S(1)}, f32[512]{0:T(512)}, u32[]{:S(2)}) copy-start(f32[512]{0:T(512)} %param.41) | copy-start | bytes 6148
  1.3 77.5 %copy-start.6 = (f32[512]{0:T(512)S(1)}, f32[512]{0:T(512)}, u32[]{:S(2)}) copy-start(f32[512]{0:T(512)} %param.42) | copy-start | bytes 6148
  1.3 77.5 %copy-start.7 = (f32[512]{0:T(512)S(1)}, f32[512]{0:T(512)}, u32[]{:S(2)}) copy-start(f32[512]{0:T(512)} %param.43) | copy-start | bytes 6148
  1.3 77.5 %copy-start.8 = (f32[512]{0:T(512)S(1)}, f32[512]{0:T(512)}, u32[]{:S(2)}) copy-start(f32[512]{0:T(512)} %param.44) | copy-start | bytes 6148
  71.5 20.7 %collective-permute-start = (bf16[16,512]{1,0:T(8,128)(2,1)S(1)}, bf16[16,512]{1,0:T(8,128)(2,1)S(1)}, u32[]{:S(2)}, u32[]{:S(2)}) collective-permute-start(bf16[16,512]{1,0:T(8,128)(2,1)S(1)} %slice.81), channel_id=1, source_target_pairs={{0,2},{2,4},{4,6},{6,8},{8,10},{10,12},{12,14},{14,16},{16,18},{18... | collective-permute-start | bytes 49160 | tf_op jit(solution)/shard_map/ppermute | solution.py:52
  77.5 0.7 copy-start.3
  77.5 0.7 copy-start.2
  78.8 0.7 copy-start.4
  78.8 0.7 copy-start.1
  92.3 1.4 copy-start

commit v3 on v2

--- a/solution.py
+++ b/solution.py
@@ -59,7 +59,7 @@
     )
 
 
-def project_kernel(n, group, pieces, tok_ref, norm_ref, *args):
+def project_kernel(n, group, pieces, tok_ref, scale_ref, bias_ref, *args):
     mats = args[:7]
     (oa_ref, op_ref, out_ref, ow_ref, wown, nall, wall, res, got, asm_sem, own_sem,
      ns, nr, ws, wr, us, ur, ds, dr, rs, rr, oas, oar, ops, opr) = args[7:]
@@ -116,59 +116,55 @@
         slot = nall.at[row_slot(at, rows)]
         return remote(slot, slot, ns.at[j], nr.at[j], base + at)
 
-    def block(index):
-        return wall.at[row_slot(index, group * deep)]
+    def block(index, j):
+        return wall.at[row_slot(index * group + lax.rem(lo + group - j, group), deep)]
 
     for j in range(1, group):
         w_copy(j).start()
     own_w = pltpu.make_async_copy(wown.at[lo], wall.at[row_slot(me, deep)], own_sem.at[1])
     own_w.start()
+
+    def relay(at, sems, s, j, peer):
+        return remote(block(at, j), block(at, j), sems[0].at[s * group + j],
+                      sems[1].at[s * group + j], peer)
+
+    def landed(s, j):
+        @pl.when(hi - 1 - s >= 0)
+        def _():
+            relay(hi - 1 - s, (us, ur), s, j, me - group).wait_recv()
+
+        @pl.when(hi + 1 + s < groups)
+        def _():
+            relay(hi + 1 + s, (ds, dr), s, j, me + group).wait_recv()
+
+    def sends(s, j, act):
+        @pl.when((hi - s >= 0) & (hi + 1 < groups))
+        def _():
+            act(relay(hi - s, (us, ur), s, j, me + group))
+
+        @pl.when((hi + s < groups) & (hi >= 1))
+        def _():
+            act(relay(hi + s, (ds, dr), s, j, me - group))
+
+    own_w.wait()
+    if groups > 1:
+        sends(0, 0, lambda c: c.start())
     x = tok_ref[...].astype(f32)
     off = x - jnp.mean(x, axis=1, keepdims=True)
     spread = jnp.mean(off * off, axis=1, keepdims=True)
     nall[row_slot(lo, rows), :] = (
-        off * lax.rsqrt(spread + 1e-5) * norm_ref[0:1] + norm_ref[1:2]
+        off * lax.rsqrt(spread + 1e-5) * scale_ref[...] + bias_ref[...]
     ).astype(bf16)
     for j in range(1, group):
         n_copy(j).start()
-    own_w.wait()
-    for j in range(1, group):
-        w_land(j).wait_recv()
-
-    def up(s):
-        return remote(block(hi - s), block(hi - s), us.at[s], ur.at[s], me + group)
-
-    def up_land(s):
-        return remote(block(hi - 1 - s), block(hi - 1 - s), us.at[s], ur.at[s], me - group)
-
-    def down(s):
-        return remote(block(hi + s), block(hi + s), ds.at[s], dr.at[s], me - group)
-
-    def down_land(s):
-        return remote(block(hi + 1 + s), block(hi + 1 + s), ds.at[s], dr.at[s], me + group)
-
-    def landed(s):
-        @pl.when(hi - 1 - s >= 0)
-        def _():
-            up_land(s).wait_recv()
-
-        @pl.when(hi + 1 + s < groups)
-        def _():
-            down_land(s).wait_recv()
-
-    def sends(s, act):
-        @pl.when((hi - s >= 0) & (hi + 1 < groups))
-        def _():
-            act(up(s))
-
-        @pl.when((hi + s < groups) & (hi >= 1))
-        def _():
-            act(down(s))
-
-    for s in range(groups - 1):
-        if s > 0:
-            landed(s - 1)
-        sends(s, lambda c: c.start())
+    for s in range(max(groups - 1, 1)):
+        for j in range(group):
+            if s == 0 and j > 0:
+                w_land(j).wait_recv()
+            if s > 0:
+                landed(s - 1, j)
+            if s < groups - 1 and s + j > 0:
+                sends(s, j, lambda c: c.start())
 
     def o_copies(j):
         return (
@@ -189,7 +185,8 @@
     for j in range(1, group):
         n_land(j).wait_recv()
     if groups > 1:
-        landed(groups - 2)
+        for j in range(group):
+            landed(groups - 2, j)
     weights = wall[...]
 
     def r_copy(j):
@@ -207,7 +204,8 @@
         n_copy(j).wait_send()
         w_copy(j).wait_send()
     for s in range(groups - 1):
-        sends(s, lambda c: c.wait_send())
+        for j in range(group):
+            sends(s, j, lambda c: c.wait_send())
     for j in range(1, group):
         r_copy(j).wait_send()
         r_copy(j).wait_recv()
@@ -222,7 +220,7 @@
             c.wait_recv()
 
 
-def project(tokens, norm, mats, out_attn, out_pool, n, group):
+def project(tokens, scale, bias, mats, out_attn, out_pool, n, group):
     rows, width = tokens.shape
     deep = mats[0].shape[0]
     total = sum(m.shape[1] for m in mats)
@@ -248,7 +246,7 @@
             jax.ShapeDtypeStruct((rows, group * wide), bf16),
             jax.ShapeDtypeStruct((groups, mix + pool, cpc), bf16),
         ],
-        in_specs=[vm, vm] + [pl.BlockSpec(memory_space=pl.ANY)] * len(mats) + [vm, vm],
+        in_specs=[vm, vm, vm] + [pl.BlockSpec(memory_space=pl.ANY)] * len(mats) + [vm, vm],
         out_specs=[vm, vm],
         scratch_shapes=[
             pltpu.VMEM((group, deep, wide), bf16),
@@ -257,13 +255,13 @@
             pltpu.VMEM((group, rows, wide), bf16),
             pltpu.VMEM((group, rows, wide), bf16),
             dma((len(pieces),)), dma((4,)),
-        ] + [dma((group,))] * 4 + [dma((groups,))] * 4 + [dma((group,))] * 2 + [dma((groups,))] * 4,
+        ] + [dma((group,))] * 4 + [dma((groups * group,))] * 4 + [dma((group,))] * 2 + [dma((groups,))] * 4,
         compiler_params=pltpu.CompilerParams(
             collective_id=0, has_side_effects=True, vmem_limit_bytes=VMEM_LIMIT
         ),
         cost_estimate=pl.CostEstimate(flops=10**11, bytes_accessed=10**7, transcendentals=0),
         name="project",
-    )(tokens, norm, *mats, out_attn, out_pool)
+    )(tokens, scale[None], bias[None], *mats, out_attn, out_pool)
 
 
 def halves(parts):
@@ -628,7 +626,7 @@
         gate_input_weight, decay_input_weight, rate_input_weight,
     )
     proj, out_rows = project(
-        tokens, jnp.stack([input_norm_scale, input_norm_bias]), mats,
+        tokens, input_norm_scale, input_norm_bias, mats,
         output_attention_rows, output_pooling_rows, n, group,
     )
     pool_in = proj[:, 3 * mix_width:4 * mix_width]

time: 164 us -> 156 us (0.951)
  Pallas kernels: 148 us -> 138 us
    pallas_call x1, Pallas kernels: 69.5 us -> 62.2 us  [project(): pl.pallas_call(functools.partial(project_kernel, n, group, tuple(pieces))...]
    pallas_call x1, Pallas kernels: 67 us -> 65.1 us  [chain(): pl.pallas_call(functools.partial(chain_kernel, n, group, m), out_shape=ja...]
where the time goes in v3:
time: 156 us; the launch traced here: 154 us
  Pallas kernels  138 us (88%)
  starting transfers between devices  6.78 us (4%)
  local copies, waits for them, and re-layouts  5.31 us (3%)
  other arithmetic  2.68 us (2%)
    pallas_call x1, Pallas kernels, chain(): pl.pallas_call(functools.partial(chain_kernel, n, group, m), out_shape=ja...  65.1 us
    pallas_call x1, Pallas kernels, project(): pl.pallas_call(functools.partial(project_kernel, n, group, tuple(pieces))...  62.2 us
    pallas_call x1, Pallas kernels, recur(): pl.pallas_call(functools.partial(recur_kernel, math.gcd(span_most, T)), g...  11.2 us
    ppermute x1, starting transfers between devices, passed_along(): lax.ppermute(value, axis, [(source, source + steps) for source in range(l...  6.78 us
  transfers between devices with their start and end apart: 1, of which 0 were waited for; matrix products, arithmetic and copies ran while one was open for 1% of the time, Pallas kernels for 7%

profile of v3, /device:TPU:11, one launch (start us, length us, event | category | flops | bytes accessed | tf_op | source)
XLA Modules:
  0.0 154.0 jit_solution(4640049748502447845)
XLA Ops:
  0.0 0.0 copy-start.5
  0.0 0.0 copy-start.6
  0.0 0.0 copy-start.7
  0.0 0.0 copy-start.8
  0.0 62.2 %project.1 = (bf16[128,2560]{1,0:T(8,128)(2,1)}, bf16[4,1024,128]{2,1,0:T(8,128)(2,1)}) custom-call(bf16[128,2048]{1,0:T(8,128)(2,1)} %tok_ref.1, f32[1,2048]{1,0:T(1,128)} %bitcast.32, f32[1,2048]{1,0:T(1,128)} %bitcast.33, bf16[128,512]{1,0:T(8,128)(2,1)} %args_0_.4, bf16[128,512]{1,0:T(8,128)(2,1)} %args_1_.4, bf16[128,512]{1,0:T(8,128)(2,1)} %args_2_.4, ...), custom_call_target="tpu_custom_call" | custom-call | flops 99999997952 | bytes 10000000 | tf_op jit(solution)/shard_map/project/pallas_call | solution.py:243
  62.2 0.7 slice.81
  62.9 6.8 %collective-permute-start = (bf16[16,512]{1,0:T(8,128)(2,1)S(1)}, bf16[16,512]{1,0:T(8,128)(2,1)S(1)}, u32[]{:S(2)}, u32[]{:S(2)}) collective-permute-start(bf16[16,512]{1,0:T(8,128)(2,1)S(1)} %slice.81), channel_id=1, source_target_pairs={{0,2},{2,4},{4,6},{6,8},{8,10},{10,12},{12,14},{14,16},{16,18},{18... | collective-permute-start | bytes 49160 | tf_op jit(solution)/shard_map/ppermute | solution.py:52
  69.8 0.0 copy-start.3
  69.8 0.0 copy-start.2
  69.8 0.7 copy-done.3
  70.5 0.0 copy-done.2
  70.5 0.6 pad_maximum_fusion.vec_ref
  71.1 0.0 copy-done.5
  71.1 0.0 copy-done.6
  71.1 0.0 copy-done.7
  71.1 0.0 copy-done.8
  71.1 0.6 copy-done.4
  71.7 0.0 copy-done.1
  71.8 0.6 stack.37.vec_ref
  72.4 11.2 %recur.1 = (f32[128,512]{1,0:T(8,128)}, f32[128,512]{1,0:T(8,128)}, f32[128,512]{1,0:T(8,128)}, f32[128,512]{1,0:T(8,128)}, bf16[8,128,64]{2,1,0:T(8,128)(2,1)}) custom-call(bf16[128,2560]{1,0:T(8,128)(2,1)} %get-tuple-element.12.q_ref.k_ref.v_ref.gl_ref.dl_ref.rl_ref, bf16[128,2560]{1,0:T(8,128)(2,1)} %get-tuple-element.12.q_ref.k_ref.v_ref.gl_ref.dl_ref.rl_ref, ...), custom_call_target="tpu_custom_call" | custom-call | flops 60000002048 | bytes 10000000 | tf_op jit(solution)/shard_map/recur/pallas_call | solution.py:401
  83.6 0.9 slice.82
  84.5 0.0 collective-permute-done
  84.6 0.0 copy-start
  84.6 1.3 fusion.4
  85.9 0.0 copy-done
  85.9 0.1 fusion.11
  86.1 0.1 fusion.5
  86.2 0.1 fusion.7
  86.3 0.1 fusion.9
  86.5 0.7 fusion.3.pool_ref
  87.1 65.1 %chain.1 = bf16[64,2048]{1,0:T(8,128)(2,1)} custom-call(f32[128,512]{1,0:T(8,128)} %get-tuple-element.13.yl_ref, f32[128,512]{1,0:T(8,128)} %get-tuple-element.14.ym_ref, f32[128,512]{1,0:T(8,128)} %get-tuple-element.15.bonus_ref, f32[128,512]{1,0:T(8,128)} %get-tuple-element.16.gate_ref, f32[2,512]{1,0:T(2,128)} %pad_maximum_fusion.vec_ref, ...), custom_call_target="tpu_custom_call" | custom-call | flops 40000000000 | bytes 10000000 | tf_op jit(solution)/shard_map/chain/pallas_call | solution.py:547
  152.3 1.7 %copy.37 = bf16[64,2048]{1,0:T(8,128)(2,1)} copy(bf16[64,2048]{1,0:T(8,128)(2,1)} %chain.1) | data formatting | bytes 524288
  (7 shorter events, 0.1 us)
Async XLA Ops:
  0.0 71.1 %copy-start.5 = (f32[512]{0:T(512)S(1)}, f32[512]{0:T(512)}, u32[]{:S(2)}) copy-start(f32[512]{0:T(512)} %param.41) | copy-start | bytes 6148
  0.0 71.1 %copy-start.6 = (f32[512]{0:T(512)S(1)}, f32[512]{0:T(512)}, u32[]{:S(2)}) copy-start(f32[512]{0:T(512)} %param.42) | copy-start | bytes 6148
  0.0 71.1 %copy-start.7 = (f32[512]{0:T(512)S(1)}, f32[512]{0:T(512)}, u32[]{:S(2)}) copy-start(f32[512]{0:T(512)} %param.43) | copy-start | bytes 6148
  0.0 71.1 %copy-start.8 = (f32[512]{0:T(512)S(1)}, f32[512]{0:T(512)}, u32[]{:S(2)}) copy-start(f32[512]{0:T(512)} %param.44) | copy-start | bytes 6148
  62.9 21.6 %collective-permute-start = (bf16[16,512]{1,0:T(8,128)(2,1)S(1)}, bf16[16,512]{1,0:T(8,128)(2,1)S(1)}, u32[]{:S(2)}, u32[]{:S(2)}) collective-permute-start(bf16[16,512]{1,0:T(8,128)(2,1)S(1)} %slice.81), channel_id=1, source_target_pairs={{0,2},{2,4},{4,6},{6,8},{8,10},{10,12},{12,14},{14,16},{16,18},{18... | collective-permute-start | bytes 49160 | tf_op jit(solution)/shard_map/ppermute | solution.py:52
  69.8 0.7 copy-start.3
  69.8 0.7 copy-start.2
  71.1 0.7 copy-start.4
  71.1 0.7 copy-start.1
  84.6 1.4 copy-start
